TPU v7x, 32 devices: a whole 2x2x4 slice. The times are simulated.
32 devices in a mesh: fs: 4 (over z), rep: 4 (over y, x), tp: 2 (over core).
Axes of the slice: x: 2, y: 2, z: 4, core: 2. Of those that a mesh axis runs over, the one named last changes fastest.
Arguments:
- attention_input: bfloat16 [12288, 2048], P(('fs', 'rep')), may hold values from -6 to 6
- query_cotangent: bfloat16 [12288, 1024], P(('fs', 'rep'), 'tp'), may hold values from -15 to 15
- gate_cotangent: float32 [16, 12288], P('tp', ('fs', 'rep')), may hold values from -6 to 6
- gate_totals: float32 [16, 12288], P('tp', ('fs', 'rep')), may hold values from -2304 to 0, as said below
- projector: bfloat16 [2048, 256], P('fs'), may hold values from -1 to 1
- query_master: float32 [2048, 1024], P('fs', 'tp'), may hold values from -0.125 to 0.125
- lowrank_mean: float32 [256, 1024], P('rep', 'tp'), may hold values from -32 to 32
- lowrank_square: float32 [256, 1024], P('rep', 'tp'), may hold values from 0.05 to 2
- gating_mean: float32 [16, 2048], P('tp'), may hold values from -1.8 to 1.8
- gating_square: float32 [16, 2048], P('tp'), may hold values from 0.01 to 1
Outputs:
- query_update: float32 [2048, 1024], P('fs', 'tp')
- query_renewed: float32 [2048, 1024], P('fs', 'tp')
- query_copy: bfloat16 [2048, 1024], P('fs', 'tp')
- mean_after: float32 [256, 1024], P('rep', 'tp')
- square_after: float32 [256, 1024], P('rep', 'tp')
- gating_update: float32 [16, 2048], P('tp')
- gating_average: float32 [16, 2048], P('tp')
- gating_energy: float32 [16, 2048], P('tp')
Inputs may be any that keep to these rules, and one draw needn't show every extreme that they name: `gate_totals`: within each sequence of 768 positions, a running sum of negative log gates, so successive differences are negative.
All inputs are finite; a program needn't handle non-finite values.
Results may differ from a plain program's by a relative error of at most 0.0044.
The roundings to bfloat16 on the way count: a program that leaves them out, or rounds other values in their place, can miss the bound.
Values may be sent and summed in bfloat16 or wider, within the bound.
A program may use at most 64 MiB of HBM per device.

v0:
```python
import functools

import jax
import jax.numpy as jnp
from jax import lax
from jax.experimental import pallas as pl
from jax.experimental.pallas import tpu as pltpu
from jax.sharding import PartitionSpec as P

BETA_ONE = 0.9
BETA_TWO = 0.95
STEP_RATE = 0.01
EPSILON = 1e-08
NORM_FLOOR = 1e-06


PIECES = 4
VMEM_GRANT = 62 * 1024 * 1024
MESH = pl.DeviceIdType.MESH
CONTRACT = (((0,), (0,)), ((), ()))


def collective_form(
    attention_input,
    query_cotangent,
    gate_cotangent,
    gate_totals,
    projector,
    query_master,
    lowrank_mean,
    lowrank_square,
    gating_mean,
    gating_square,
):
    tokens_all = attention_input.shape[0] * lax.axis_size("fs") * lax.axis_size("rep")
    norming = 1.0 / tokens_all**0.5
    contract = (((0,), (0,)), ((), ()))
    earlier = jnp.concatenate(
        [jnp.zeros((gate_totals.shape[0], 1), jnp.float32), gate_totals[:, :-1]], axis=1
    )
    gate_logarithm = gate_totals - earlier
    trailing = lax.cumsum(gate_cotangent, axis=1, reverse=True)
    gate_signal = (trailing * -jnp.expm1(gate_logarithm)).astype(jnp.bfloat16)
    gate_partial = jnp.dot(gate_signal, attention_input, preferred_element_type=jnp.float32)
    forget_gradient = lax.psum(gate_partial, ("fs", "rep")) * norming
    thin_rows = lax.psum_scatter(
        lax.dot_general(
            attention_input, query_cotangent, contract, preferred_element_type=jnp.float32
        ),
        ("fs", "rep"),
        scatter_dimension=0,
        tiled=True,
    )
    gradient = lax.all_gather(thin_rows, "rep", axis=0, tiled=True) * norming
    rank_rows = lowrank_mean.shape[0]
    own_factor = lax.dynamic_slice_in_dim(
        projector, lax.axis_index("rep") * rank_rows, rank_rows, 1
    ).astype(jnp.float32)
    rank_partial = lax.dot_general(
        own_factor,
        gradient,
        contract,
        precision=lax.Precision.HIGHEST,
        preferred_element_type=jnp.float32,
    )
    projected = lax.psum(rank_partial, "fs")
    mean_after = BETA_ONE * lowrank_mean + (1.0 - BETA_ONE) * projected
    square_after = BETA_TWO * lowrank_square + (1.0 - BETA_TWO) * projected * projected
    direction = mean_after / (jnp.sqrt(square_after) + EPSILON)
    direction_squares, projected_squares = lax.psum(
        (jnp.sum(direction * direction), jnp.sum(projected * projected)), ("rep", "tp")
    )
    balance = jnp.sqrt(direction_squares / (projected_squares + NORM_FLOOR))
    blended = (direction - balance * projected).astype(jnp.bfloat16)
    lifted = jnp.dot(
        projector,
        lax.all_gather(blended, "rep", axis=0, tiled=True),
        preferred_element_type=jnp.float32,
    )
    query_update = lifted + balance * gradient
    query_renewed = query_master - STEP_RATE * query_update
    query_copy = query_renewed.astype(jnp.bfloat16)
    gating_average = BETA_ONE * gating_mean + (1.0 - BETA_ONE) * forget_gradient
    gating_energy = BETA_TWO * gating_square + (1.0 - BETA_TWO) * forget_gradient * forget_gradient
    gating_update = gating_average / (jnp.sqrt(gating_energy) + EPSILON)
    return (
        query_update,
        query_renewed,
        query_copy,
        mean_after,
        square_after,
        gating_update,
        gating_average,
        gating_energy,
    )


def fused_kernel(
    nf, nr, nt,
    x_hbm, c_hbm, gc_ref, gt_ref, pj_ref, lm_ref, ls_ref,
    g_all, h_all, balance_ref, projected_ref, rd_all,
    x_ref, c_ref,
    a_send, a_recv, a_own, b_send, b_recv, g_ref,
    d_part, d_recv, e_part, e_recv, e_own, proj, f_send, f_recv,
    ra_send, ra_recv, rb_part, rb_recv, rc_all,
    send_sem, recv_sem, load_sem,
):
    f, r, t = lax.axis_index("fs"), lax.axis_index("rep"), lax.axis_index("tp")
    tokens, width = x_ref.shape
    cols = c_ref.shape[1]
    piece = cols // PIECES
    thin = width // (nf * nr)
    norming = 1.0 / (tokens * nf * nr) ** 0.5
    started = []

    def columns(owner_r, owner_f):
        return pl.ds(pl.multiple_of((owner_f * nr + owner_r) * thin, thin), thin)

    load_c = pltpu.make_async_copy(c_hbm, c_ref, load_sem.at[nr * nf])
    load_c.start()
    loads = {}
    for k in list(range(1, nr)) + [0]:
        for j in range(nf):
            where = columns(lax.rem(r + k, nr), j)
            loads[k, j] = pltpu.make_async_copy(
                x_hbm.at[:, where], x_ref.at[:, where], load_sem.at[k * nf + j]
            )
            loads[k, j].start()

    def at(df, dr, dt):
        return (lax.rem(f + df, nf), lax.rem(r + dr, nr), lax.rem(t + dt, nt))

    def send(src, dst, where):
        slot = len(started)
        copy = pltpu.make_async_remote_copy(
            src_ref=src, dst_ref=dst, send_sem=send_sem.at[slot], recv_sem=recv_sem.at[slot],
            device_id=where, device_id_type=MESH,
        )
        copy.start()
        started.append(copy)
        return copy

    reps = list(range(1, nr))
    fss = list(range(1, nf))
    rest = [(dr, dt) for dr in range(nr) for dt in range(nt) if dr or dt]
    peers = [at(df, 0, 0) for df in fss] + [at(0, dr, dt) for dr, dt in rest]
    barrier = pltpu.get_barrier_semaphore()
    for peer in peers:
        pl.semaphore_signal(barrier, inc=1, device_id=peer, device_id_type=MESH)

    load_c.wait()

    def block(k, j):
        loads[k, j].wait()
        return lax.dot_general(
            x_ref[:, columns(lax.rem(r + k, nr), j)], c_ref[...], CONTRACT,
            preferred_element_type=jnp.float32,
        )

    a_copies = [[None] * (nr - 1) for _ in range(PIECES)]
    for k in reps:
        for j in range(nf):
            value = block(k, j).astype(jnp.bfloat16)
            for p in range(PIECES):
                a_send[p, k - 1, j] = value[:, p * piece : (p + 1) * piece]
        if k == reps[0]:
            pl.semaphore_wait(barrier, len(peers))
        a_copies[0][k - 1] = send(a_send.at[0, k - 1], a_recv.at[0, k - 1], at(0, k, 0))
    for p in range(1, PIECES):
        for k in reps:
            a_copies[p][k - 1] = send(a_send.at[p, k - 1], a_recv.at[p, k - 1], at(0, k, 0))
    for j in range(nf):
        a_own[j] = block(0, j)

    lanes = 128
    lower = lax.broadcasted_iota(jnp.int32, (lanes, lanes), 0)
    upper = lax.broadcasted_iota(jnp.int32, (lanes, lanes), 1)
    later = (lower >= upper).astype(jnp.float32)
    carry = jnp.zeros((gc_ref.shape[0], 1), jnp.float32)
    signals = []
    totals = gt_ref[...]
    first = lax.broadcasted_iota(jnp.int32, totals.shape, 1) == 0
    gate_logarithm = totals - jnp.where(first, 0.0, pltpu.roll(totals, 1, 1))
    for i in reversed(range(tokens // lanes)):
        window = slice(i * lanes, (i + 1) * lanes)
        own = gc_ref[:, window]
        trailing = carry + jnp.dot(
            own, later, precision=lax.Precision.HIGHEST, preferred_element_type=jnp.float32
        )
        carry = carry + jnp.sum(own, axis=1, keepdims=True)
        signals.append(trailing)
    trailing = jnp.concatenate(signals[::-1], axis=1)
    series = jnp.ones_like(gate_logarithm)
    for i in range(8, 1, -1):
        series = 1.0 + gate_logarithm * series / i
    opening = jnp.where(
        gate_logarithm > -0.25, -gate_logarithm * series, 1.0 - jnp.exp(gate_logarithm)
    )
    gate_signal = (trailing * opening).astype(jnp.bfloat16)
    gate_partial = jnp.dot(gate_signal, x_ref[...], preferred_element_type=jnp.float32)
    for i in range(nr):
        for j in range(nf):
            start = (i * nf + j) * thin
            ra_send[i, j] = gate_partial[:, start : start + thin]
    ra = [send(ra_send.at[lax.rem(r + k, nr)], ra_recv.at[k - 1], at(0, k, 0)) for k in reps]

    b_copies = []
    for p in range(PIECES):
        window = slice(p * piece, (p + 1) * piece)
        for copy in a_copies[p]:
            copy.wait_recv()

        def summed(j):
            total = a_own[j, :, window]
            for k in reps:
                total = total + a_recv[p, k - 1, j].astype(jnp.float32)
            return total

        row = []
        for k in fss:
            b_send[p, k - 1] = summed(lax.rem(f + k, nf)).astype(jnp.bfloat16)
            row.append(send(b_send.at[p, k - 1], b_recv.at[p, k - 1], at(k, 0, 0)))
        g_ref[:, window] = summed(f)
        b_copies.append(row)
    for copy in ra:
        copy.wait_recv()
    gate_rows = ra_send[r]
    for k in reps:
        gate_rows = gate_rows + ra_recv[k - 1]
    rb_part[...] = gate_rows
    rb = [send(rb_part.at[lax.rem(f + k, nf)], rb_recv.at[k - 1], at(k, 0, 0)) for k in fss]

    for p in range(PIECES):
        window = slice(p * piece, (p + 1) * piece)
        for copy in b_copies[p]:
            copy.wait_recv()
        total = g_ref[:, window]
        for k in fss:
            total = total + b_recv[p, k - 1].astype(jnp.float32)
        g_ref[:, window] = total * norming
    gradient = g_ref[...]
    g_all[r] = gradient.astype(jnp.bfloat16)
    factor = pj_ref[pl.ds(pl.multiple_of(r * thin, thin), thin), :].astype(jnp.float32)
    partial = lax.dot_general(
        factor, gradient, CONTRACT, precision=lax.Precision.HIGHEST,
        preferred_element_type=jnp.float32,
    )
    d_part[...] = partial.reshape(d_part.shape)
    d = [send(d_part.at[lax.rem(r + k, nr)], d_recv.at[k - 1], at(0, k, 0)) for k in reps]

    for copy in rb:
        copy.wait_recv()
    gate_block = rb_part[f]
    for k in fss:
        gate_block = gate_block + rb_recv[k - 1]
    rc_all[f] = gate_block * norming
    rc = [send(rc_all.at[f], rc_all.at[f], at(k, 0, 0)) for k in fss]

    for copy in d:
        copy.wait_recv()
    c = [send(g_all.at[r], g_all.at[r], at(0, k, 0)) for k in reps]
    total = d_part[r]
    for k in reps:
        total = total + d_recv[k - 1]
    e_part[...] = total.reshape(e_part.shape)
    e = [send(e_part.at[lax.rem(f + k, nf)], e_recv.at[k - 1], at(k, 0, 0)) for k in fss]
    for copy in e:
        copy.wait_recv()
    total = e_part[f]
    for k in fss:
        total = total + e_recv[k - 1]
    proj[f] = total
    e2 = [send(proj.at[f], proj.at[f], at(k, 0, 0)) for k in fss]

    for copy in rc:
        copy.wait_recv()
    rd_all[r] = rc_all[...]
    rd = [send(rc_all, rd_all.at[r], at(0, k, 0)) for k in reps]

    for copy in e2:
        copy.wait_recv()
    projected = proj[...].reshape(lm_ref.shape)
    mean_after = BETA_ONE * lm_ref[...] + (1.0 - BETA_ONE) * projected
    square_after = BETA_TWO * ls_ref[...] + (1.0 - BETA_TWO) * projected * projected
    direction = mean_after / (jnp.sqrt(square_after) + EPSILON)
    f_send[0] = jnp.full(f_send.shape[1:], jnp.sum(direction * direction))
    f_send[1] = jnp.full(f_send.shape[1:], jnp.sum(projected * projected))
    fc = [send(f_send, f_recv.at[i], at(0, dr, dt)) for i, (dr, dt) in enumerate(rest)]
    projected_ref[...] = projected
    for copy in fc:
        copy.wait_recv()
    sums = f_send[...]
    for i in range(len(rest)):
        sums = sums + f_recv[i]
    ratio = jnp.sqrt(sums[0] / (sums[1] + NORM_FLOOR))
    balance_ref[...] = ratio
    balance = ratio[:1, :1]
    h_all[r] = (direction - balance * projected).astype(jnp.bfloat16)
    h = [send(h_all.at[r], h_all.at[r], at(0, k, 0)) for k in reps]

    for copy in rd + c + h:
        copy.wait_recv()
    for copy in started:
        copy.wait_send()


def closing_kernel(
    g_ref, h_ref, balance_ref, projected_ref, gate_ref, pj_ref, qm_ref, lm_ref, ls_ref, gm_ref, gq_ref,
    qu_ref, qr_ref, qc_ref, ma_ref, sa_ref, gu_ref, ga_ref, ge_ref,
):
    lifted = jnp.dot(
        pj_ref[...], h_ref[...].reshape(pj_ref.shape[1], qm_ref.shape[1]),
        preferred_element_type=jnp.float32,
    )
    query_update = lifted + balance_ref[:1, :1] * g_ref[0].astype(jnp.float32)
    query_renewed = qm_ref[...] - STEP_RATE * query_update
    qu_ref[...] = query_update
    qr_ref[...] = query_renewed
    qc_ref[...] = query_renewed.astype(jnp.bfloat16)

    @pl.when(pl.program_id(0) == 0)
    def _():
        projected = projected_ref[...]
        ma_ref[...] = BETA_ONE * lm_ref[...] + (1.0 - BETA_ONE) * projected
        sa_ref[...] = BETA_TWO * ls_ref[...] + (1.0 - BETA_TWO) * projected * projected
        nr, nf, _, thin = gate_ref.shape
        for i in range(nr):
            for j in range(nf):
                window = slice((i * nf + j) * thin, (i * nf + j + 1) * thin)
                forget_gradient = gate_ref[i, j]
                average = BETA_ONE * gm_ref[:, window] + (1.0 - BETA_ONE) * forget_gradient
                energy = (
                    BETA_TWO * gq_ref[:, window]
                    + (1.0 - BETA_TWO) * forget_gradient * forget_gradient
                )
                ga_ref[:, window] = average
                ge_ref[:, window] = energy
                gu_ref[:, window] = average / (jnp.sqrt(energy) + EPSILON)


def per_device(nf, nr, nt, *args):
    x, c, gc, _, pj, qm, lm, ls, gm, gq = args
    width, cols, rank_rows, heads = x.shape[1], c.shape[1], lm.shape[0], gc.shape[0]
    thin = width // (nf * nr)
    fits = (
        width % (nf * nr * 128) == 0 and rank_rows % (nf * 16) == 0
        and cols % (PIECES * 128) == 0 and heads % 8 == 0 and min(nf, nr) > 1
        and x.shape[0] % 128 == 0
    )
    if not fits:
        return collective_form(*args)
    piece, bf, fl = cols // PIECES, jnp.bfloat16, jnp.float32
    scratch = [
        (x.shape, bf), (c.shape, bf),
        ((PIECES, nr - 1, nf, thin, piece), bf), ((PIECES, nr - 1, nf, thin, piece), bf),
        ((nf, thin, cols), fl), ((PIECES, nf - 1, thin, piece), bf),
        ((PIECES, nf - 1, thin, piece), bf), ((thin, cols), fl),
        ((nr, rank_rows, cols), fl), ((nr - 1, rank_rows, cols), fl),
        ((nf, rank_rows // nf, cols), fl), ((nf - 1, rank_rows // nf, cols), fl),
        ((8, 128), fl), ((nf, rank_rows // nf, cols), fl),
        ((2, 8, 128), fl), ((nr * nt - 1, 2, 8, 128), fl),
        ((nr, nf, heads, thin), fl), ((nr - 1, nf, heads, thin), fl),
        ((nf, heads, thin), fl), ((nf - 1, heads, thin), fl),
        ((nf, heads, thin), fl),
    ]
    copies = (nr - 1) * (PIECES + 5) + (nf - 1) * (PIECES + 4) + nr * nt - 1
    outs = [
        (qm.shape, fl), (qm.shape, fl), (qm.shape, bf), (lm.shape, fl), (lm.shape, fl),
        (gm.shape, fl), (gm.shape, fl), (gm.shape, fl),
    ]
    between = [
        ((nr, thin, cols), bf), ((nr, rank_rows, cols), bf), ((8, 128), fl), (lm.shape, fl),
        ((nr, nf, heads, thin), fl),
    ]
    vmem = pl.BlockSpec(memory_space=pltpu.VMEM)
    hbm = pl.BlockSpec(memory_space=pl.ANY)
    passed = pl.pallas_call(
        functools.partial(fused_kernel, nf, nr, nt),
        out_shape=tuple(jax.ShapeDtypeStruct(*o) for o in between),
        in_specs=[hbm] * 2 + [vmem] * 5,
        out_specs=(vmem,) * len(between),
        scratch_shapes=[pltpu.VMEM(*v) for v in scratch]
        + [pltpu.SemaphoreType.DMA((copies,)), pltpu.SemaphoreType.DMA((copies,))]
        + [pltpu.SemaphoreType.DMA((nr * nf + 1,))],
        compiler_params=pltpu.CompilerParams(
            collective_id=0, has_side_effects=True, vmem_limit_bytes=VMEM_GRANT
        ),
    )(x, c, gc, args[3], pj, lm, ls)

    def whole(shape):
        return pl.BlockSpec(shape, lambda i: (0,) * len(shape))

    def rows(width):
        return pl.BlockSpec((thin, width), lambda i: (i, 0))

    return pl.pallas_call(
        closing_kernel,
        grid=(nr,),
        out_shape=tuple(jax.ShapeDtypeStruct(*o) for o in outs),
        in_specs=[pl.BlockSpec((1, thin, cols), lambda i: (i, 0, 0))]
        + [whole(b[0]) for b in between[1:]]
        + [rows(pj.shape[1]), rows(cols), whole(lm.shape), whole(ls.shape)]
        + [whole(gm.shape), whole(gq.shape)],
        out_specs=(rows(cols),) * 3 + tuple(whole(o[0]) for o in outs[3:]),
        compiler_params=pltpu.CompilerParams(vmem_limit_bytes=VMEM_GRANT),
    )(*passed, pj, qm, lm, ls, gm, gq)


def solution(mesh):
    in_specs = (
        P(("fs", "rep"), None),
        P(("fs", "rep"), "tp"),
        P("tp", ("fs", "rep")),
        P("tp", ("fs", "rep")),
        P("fs", None),
        P("fs", "tp"),
        P("rep", "tp"),
        P("rep", "tp"),
        P("tp", None),
        P("tp", None),
    )
    out_specs = (
        P("fs", "tp"),
        P("fs", "tp"),
        P("fs", "tp"),
        P("rep", "tp"),
        P("rep", "tp"),
        P("tp", None),
        P("tp", None),
        P("tp", None),
    )
    return jax.shard_map(
        functools.partial(per_device, mesh.shape["fs"], mesh.shape["rep"], mesh.shape["tp"]),
        mesh=mesh, in_specs=in_specs, out_specs=out_specs, check_vma=False
    )
```

profile of v0, /device:TPU:0, one launch (start us, length us, event | category | flops | bytes accessed | tf_op | source)
XLA Modules:
  0.0 68.8 jit_solution(18243089156343454571)
XLA Ops:
  0.6 63.5 %shard_map.161 = (bf16[4,128,512]{2,1,0:T(8,128)(2,1)}, bf16[4,64,512]{2,1,0:T(8,128)(2,1)}, f32[8,128]{1,0:T(8,128)}, f32[64,512]{1,0:T(8,128)}, f32[4,4,8,128]{3,2,1,0:T(8,128)}) custom-call(bf16[768,2048]{1,0:T(8,128)(2,1)} %x_hbm.1, bf16[768,512]{1,0:T(8,128)(2,1)} %c_hbm.1, f32[8,768]{1,0:T(8,128)} %gc_ref.1, f32[8,768]{1,0:T(8,128)} %gt_ref.1, ...), custom_call_target="tpu_custom_call" | custom-call | tf_op jit(solution)/shard_map/pallas_call | solution.py:377
  64.1 4.7 %shard_map.162 = (f32[512,512]{1,0:T(8,128)}, f32[512,512]{1,0:T(8,128)}, bf16[512,512]{1,0:T(8,128)(2,1)}, f32[64,512]{1,0:T(8,128)}, f32[64,512]{1,0:T(8,128)}...) custom-call(bf16[4,128,512]{2,1,0:T(8,128)(2,1)} %get-tuple-element.13.g_ref, ...), custom_call_target="tpu_custom_call" | custom-call | tf_op jit(solution)/shard_map/pallas_call | solution.py:396
where the time goes:
time: 69 us; the launch traced here: 68.8 us
  Pallas kernels  68.2 us (99%)
    pallas_call x1, Pallas kernels, per_device(): pl.pallas_call(functools.partial(fused_kernel, nf, nr, nt), out_shape=tup...  63.5 us
    pallas_call x1, Pallas kernels, per_device(): pl.pallas_call(closing_kernel, grid=(nr,), out_shape=tuple((jax.ShapeDtyp...  4.72 us

commit v1 on v0

--- a/solution.py
+++ b/solution.py
@@ -15,7 +15,7 @@
 
 
 PIECES = 4
-VMEM_GRANT = 62 * 1024 * 1024
+VMEM_GRANT = 24 * 1024 * 1024
 MESH = pl.DeviceIdType.MESH
 CONTRACT = (((0,), (0,)), ((), ()))
 
@@ -373,7 +373,7 @@
         ((nr, nf, heads, thin), fl),
     ]
     vmem = pl.BlockSpec(memory_space=pltpu.VMEM)
-    hbm = pl.BlockSpec(memory_space=pl.ANY)
+    hbm = pl.BlockSpec(memory_space=pltpu.HBM)
     passed = pl.pallas_call(
         functools.partial(fused_kernel, nf, nr, nt),
         out_shape=tuple(jax.ShapeDtypeStruct(*o) for o in between),

time: 69 us -> 73.5 us (1.065)
  local copies, waits for them, and re-layouts: 0 us -> 7.26 us
  Pallas kernels: 68.2 us -> 65.2 us
    unnamed x0 -> x20, local copies, waits for them, and re-layouts: none -> 7.26 us
    pallas_call x1, Pallas kernels: 4.72 us -> 2.64 us  [per_device(): pl.pallas_call(closing_kernel, grid=(nr,), out_shape=tuple((jax.ShapeDtyp...]
    pallas_call x1, Pallas kernels: 63.5 us -> 62.5 us  [per_device(): pl.pallas_call(functools.partial(fused_kernel, nf, nr, nt), out_shape=tup...]
where the time goes in v1:
time: 73.5 us; the launch traced here: 73.1 us
  Pallas kernels  65.2 us (89%)
  local copies, waits for them, and re-layouts  7.26 us (10%)
    pallas_call x1, Pallas kernels, per_device(): pl.pallas_call(functools.partial(fused_kernel, nf, nr, nt), out_shape=tup...  62.5 us
    unnamed x20, local copies, waits for them, and re-layouts  7.26 us
    pallas_call x1, Pallas kernels, per_device(): pl.pallas_call(closing_kernel, grid=(nr,), out_shape=tuple((jax.ShapeDtyp...  2.64 us

profile of v1, /device:TPU:0, one launch (start us, length us, event | category | flops | bytes accessed | tf_op | source)
XLA Modules:
  0.0 73.1 jit_solution(6561676476812330944)
XLA Ops:
  0.6 0.0 copy-start
  0.6 1.9 %copy-done = bf16[768,2048]{1,0:T(8,128)(2,1)S(1)} copy-done((bf16[768,2048]{1,0:T(8,128)(2,1)S(1)}, bf16[768,2048]{1,0:T(8,128)(2,1)}, u32[]{:S(2)}) %copy-start) | copy-done | bytes 3145752
  2.5 0.0 copy-start.2
  2.5 0.9 %copy-done.2 = bf16[512,256]{1,0:T(8,128)(2,1)S(1)} copy-done((bf16[512,256]{1,0:T(8,128)(2,1)S(1)}, bf16[512,256]{1,0:T(8,128)(2,1)}, u32[]{:S(2)}) %copy-start.2) | copy-done | bytes 262168
  3.5 0.0 copy-start.3
  3.5 1.1 %copy-done.3 = bf16[768,512]{1,0:T(8,128)(2,1)S(1)} copy-done((bf16[768,512]{1,0:T(8,128)(2,1)S(1)}, bf16[768,512]{1,0:T(8,128)(2,1)}, u32[]{:S(2)}) %copy-start.3) | copy-done | bytes 786456
  4.6 0.0 copy-start.4
  4.6 0.9 %copy-done.4 = f32[64,512]{1,0:T(8,128)S(1)} copy-done((f32[64,512]{1,0:T(8,128)S(1)}, f32[64,512]{1,0:T(8,128)}, u32[]{:S(2)}) %copy-start.4) | copy-done | bytes 131096
  5.5 0.0 copy-start.5
  5.5 0.9 %copy-done.5 = f32[64,512]{1,0:T(8,128)S(1)} copy-done((f32[64,512]{1,0:T(8,128)S(1)}, f32[64,512]{1,0:T(8,128)}, u32[]{:S(2)}) %copy-start.5) | copy-done | bytes 131096
  6.4 0.0 copy-start.8
  6.4 0.7 %copy-done.8 = f32[8,768]{1,0:T(8,128)S(1)} copy-done((f32[8,768]{1,0:T(8,128)S(1)}, f32[8,768]{1,0:T(8,128)}, u32[]{:S(2)}) %copy-start.8) | copy-done | bytes 24600
  7.2 0.0 copy-start.9
  7.2 0.7 %copy-done.9 = f32[8,768]{1,0:T(8,128)S(1)} copy-done((f32[8,768]{1,0:T(8,128)S(1)}, f32[8,768]{1,0:T(8,128)}, u32[]{:S(2)}) %copy-start.9) | copy-done | bytes 24600
  7.9 0.0 copy-start.1
  7.9 0.0 copy-start.6
  7.9 0.0 copy-start.7
  7.9 62.5 %shard_map.161 = (bf16[4,128,512]{2,1,0:T(8,128)(2,1)S(1)}, bf16[4,64,512]{2,1,0:T(8,128)(2,1)S(1)}, f32[8,128]{1,0:T(8,128)S(1)}, f32[64,512]{1,0:T(8,128)S(1)}, f32[4,4,8,128]{3,2,1,0:T(8,128)S(1)}) custom-call(bf16[768,2048]{1,0:T(8,128)(2,1)S(1)} %copy-done, bf16[768,512]{1,0:T(8,128)(2,1)S(1)} %copy-done.3, f32[8,768]{1,0:T(8,128)S(1)} %copy-done.8, ...), custom_call_target="tpu_custom_call" | custom-call | tf_op jit(solution)/shard_map/pallas_call | solution.py:377
  70.5 0.0 copy-done.1
  70.5 0.0 copy-done.6
  70.5 0.0 copy-done.7
  70.5 2.6 %shard_map.162 = (f32[512,512]{1,0:T(8,128)}, f32[512,512]{1,0:T(8,128)}, bf16[512,512]{1,0:T(8,128)(2,1)}, f32[64,512]{1,0:T(8,128)}, f32[64,512]{1,0:T(8,128)}...) custom-call(bf16[4,128,512]{2,1,0:T(8,128)(2,1)S(1)} %get-tuple-element.13.g_ref, ...), custom_call_target="tpu_custom_call" | custom-call | tf_op jit(solution)/shard_map/pallas_call | solution.py:396
Async XLA Ops:
  0.6 1.9 %copy-start = (bf16[768,2048]{1,0:T(8,128)(2,1)S(1)}, bf16[768,2048]{1,0:T(8,128)(2,1)}, u32[]{:S(2)}) copy-start(bf16[768,2048]{1,0:T(8,128)(2,1)} %x_hbm.1) | copy-start | bytes 9437188
  2.5 0.9 %copy-start.2 = (bf16[512,256]{1,0:T(8,128)(2,1)S(1)}, bf16[512,256]{1,0:T(8,128)(2,1)}, u32[]{:S(2)}) copy-start(bf16[512,256]{1,0:T(8,128)(2,1)} %pj_ref.3) | copy-start | bytes 786436
  3.5 1.1 %copy-start.3 = (bf16[768,512]{1,0:T(8,128)(2,1)S(1)}, bf16[768,512]{1,0:T(8,128)(2,1)}, u32[]{:S(2)}) copy-start(bf16[768,512]{1,0:T(8,128)(2,1)} %c_hbm.1) | copy-start | bytes 2359300
  4.6 0.9 %copy-start.4 = (f32[64,512]{1,0:T(8,128)S(1)}, f32[64,512]{1,0:T(8,128)}, u32[]{:S(2)}) copy-start(f32[64,512]{1,0:T(8,128)} %lm_ref.3) | copy-start | bytes 393220
  5.5 0.9 %copy-start.5 = (f32[64,512]{1,0:T(8,128)S(1)}, f32[64,512]{1,0:T(8,128)}, u32[]{:S(2)}) copy-start(f32[64,512]{1,0:T(8,128)} %ls_ref.3) | copy-start | bytes 393220
  6.4 0.7 %copy-start.8 = (f32[8,768]{1,0:T(8,128)S(1)}, f32[8,768]{1,0:T(8,128)}, u32[]{:S(2)}) copy-start(f32[8,768]{1,0:T(8,128)} %gc_ref.1) | copy-start | bytes 73732
  7.2 0.7 %copy-start.9 = (f32[8,768]{1,0:T(8,128)S(1)}, f32[8,768]{1,0:T(8,128)}, u32[]{:S(2)}) copy-start(f32[8,768]{1,0:T(8,128)} %gt_ref.1) | copy-start | bytes 73732
  7.9 62.6 %copy-start.1 = (f32[512,512]{1,0:T(8,128)S(1)}, f32[512,512]{1,0:T(8,128)}, u32[]{:S(2)}) copy-start(f32[512,512]{1,0:T(8,128)} %qm_ref.1) | copy-start | bytes 3145732
  7.9 62.6 %copy-start.6 = (f32[8,2048]{1,0:T(8,128)S(1)}, f32[8,2048]{1,0:T(8,128)}, u32[]{:S(2)}) copy-start(f32[8,2048]{1,0:T(8,128)} %gm_ref.1) | copy-start | bytes 196612
  7.9 62.6 %copy-start.7 = (f32[8,2048]{1,0:T(8,128)S(1)}, f32[8,2048]{1,0:T(8,128)}, u32[]{:S(2)}) copy-start(f32[8,2048]{1,0:T(8,128)} %gq_ref.1) | copy-start | bytes 196612

commit v2 on v1

--- a/solution.py
+++ b/solution.py
@@ -385,7 +385,7 @@
         compiler_params=pltpu.CompilerParams(
             collective_id=0, has_side_effects=True, vmem_limit_bytes=VMEM_GRANT
         ),
-    )(x, c, gc, args[3], pj, lm, ls)
+    )(*(pltpu.with_memory_space_constraint(v, pltpu.HBM) for v in (x, c)), gc, args[3], pj, lm, ls)
 
     def whole(shape):
         return pl.BlockSpec(shape, lambda i: (0,) * len(shape))

time: 73.5 us -> 69.5 us (0.946)
  local copies, waits for them, and re-layouts: 7.26 us -> 4.33 us
  Pallas kernels: 65.2 us -> 64.1 us
    unnamed x20 -> x22, local copies, waits for them, and re-layouts: 7.26 us -> 4.33 us
    pallas_call x1, Pallas kernels: 62.5 us -> 61.5 us  [per_device(): pl.pallas_call(functools.partial(fused_kernel, nf, nr, nt), out_shape=tup...]
where the time goes in v2:
time: 69.5 us; the launch traced here: 69.2 us
  Pallas kernels  64.1 us (92%)
  local copies, waits for them, and re-layouts  4.33 us (6%)
  between operations  0.73 us (1%)
    pallas_call x1, Pallas kernels, per_device(): pl.pallas_call(functools.partial(fused_kernel, nf, nr, nt), out_shape=tup...  61.5 us
    unnamed x22, local copies, waits for them, and re-layouts  4.33 us
    pallas_call x1, Pallas kernels, per_device(): pl.pallas_call(closing_kernel, grid=(nr,), out_shape=tuple((jax.ShapeDtyp...  2.65 us

profile of v2, /device:TPU:0, one launch (start us, length us, event | category | flops | bytes accessed | tf_op | source)
XLA Modules:
  0.0 69.2 jit_solution(4260906663101104736)
XLA Ops:
  0.6 0.0 copy-start
  0.6 0.0 copy-start.1
  0.7 1.0 %copy-done.1 = bf16[512,256]{1,0:T(8,128)(2,1)S(1)} copy-done((bf16[512,256]{1,0:T(8,128)(2,1)S(1)}, bf16[512,256]{1,0:T(8,128)(2,1)}, u32[]{:S(2)}) %copy-start.1) | copy-done | bytes 262168
  1.7 0.0 copy-start.3
  1.7 0.9 %copy-done.3 = f32[64,512]{1,0:T(8,128)S(1)} copy-done((f32[64,512]{1,0:T(8,128)S(1)}, f32[64,512]{1,0:T(8,128)}, u32[]{:S(2)}) %copy-start.3) | copy-done | bytes 131096
  2.6 0.0 copy-start.5
  2.6 0.9 %copy-done.5 = f32[64,512]{1,0:T(8,128)S(1)} copy-done((f32[64,512]{1,0:T(8,128)S(1)}, f32[64,512]{1,0:T(8,128)}, u32[]{:S(2)}) %copy-start.5) | copy-done | bytes 131096
  3.5 0.0 copy-start.9
  3.5 0.7 %copy-done.9 = f32[8,768]{1,0:T(8,128)S(1)} copy-done((f32[8,768]{1,0:T(8,128)S(1)}, f32[8,768]{1,0:T(8,128)}, u32[]{:S(2)}) %copy-start.9) | copy-done | bytes 24600
  4.2 0.0 copy-start.10
  4.2 0.7 %copy-done.10 = f32[8,768]{1,0:T(8,128)S(1)} copy-done((f32[8,768]{1,0:T(8,128)S(1)}, f32[8,768]{1,0:T(8,128)}, u32[]{:S(2)}) %copy-start.10) | copy-done | bytes 24600
  5.0 0.0 copy-start.2
  5.0 0.0 copy-start.4
  5.0 0.0 copy-start.6
  5.0 0.0 copy-start.7
  5.0 0.0 copy-start.8
  5.0 61.5 %shard_map.161 = (bf16[4,128,512]{2,1,0:T(8,128)(2,1)S(1)}, bf16[4,64,512]{2,1,0:T(8,128)(2,1)S(1)}, f32[8,128]{1,0:T(8,128)S(1)}, f32[64,512]{1,0:T(8,128)S(1)}, f32[4,4,8,128]{3,2,1,0:T(8,128)S(1)}) custom-call(bf16[768,2048]{1,0:T(8,128)(2,1)} %x_hbm.1, bf16[768,512]{1,0:T(8,128)(2,1)} %c_hbm.1, f32[8,768]{1,0:T(8,128)S(1)} %copy-done.9, ...), custom_call_target="tpu_custom_call" | custom-call | tf_op jit(solution)/shard_map/pallas_call | solution.py:377
  66.5 0.0 copy-done
  66.5 0.0 copy-done.2
  66.5 0.0 copy-done.4
  66.5 0.0 copy-done.6
  66.5 0.0 copy-done.7
  66.6 0.0 copy-done.8
  66.6 2.6 %shard_map.162 = (f32[512,512]{1,0:T(8,128)}, f32[512,512]{1,0:T(8,128)}, bf16[512,512]{1,0:T(8,128)(2,1)}, f32[64,512]{1,0:T(8,128)}, f32[64,512]{1,0:T(8,128)}...) custom-call(bf16[4,128,512]{2,1,0:T(8,128)(2,1)S(1)} %get-tuple-element.13.g_ref, ...), custom_call_target="tpu_custom_call" | custom-call | tf_op jit(solution)/shard_map/pallas_call | solution.py:396
Async XLA Ops:
  0.6 65.9 %copy-start = (f32[512,512]{1,0:T(8,128)S(1)}, f32[512,512]{1,0:T(8,128)}, u32[]{:S(2)}) copy-start(f32[512,512]{1,0:T(8,128)} %qm_ref.1) | copy-start | bytes 3145732
  0.6 1.0 %copy-start.1 = (bf16[512,256]{1,0:T(8,128)(2,1)S(1)}, bf16[512,256]{1,0:T(8,128)(2,1)}, u32[]{:S(2)}) copy-start(bf16[512,256]{1,0:T(8,128)(2,1)} %pj_ref.3) | copy-start | bytes 786436
  1.7 0.9 %copy-start.3 = (f32[64,512]{1,0:T(8,128)S(1)}, f32[64,512]{1,0:T(8,128)}, u32[]{:S(2)}) copy-start(f32[64,512]{1,0:T(8,128)} %lm_ref.3) | copy-start | bytes 393220
  2.6 0.9 %copy-start.5 = (f32[64,512]{1,0:T(8,128)S(1)}, f32[64,512]{1,0:T(8,128)}, u32[]{:S(2)}) copy-start(f32[64,512]{1,0:T(8,128)} %ls_ref.3) | copy-start | bytes 393220
  3.5 0.7 %copy-start.9 = (f32[8,768]{1,0:T(8,128)S(1)}, f32[8,768]{1,0:T(8,128)}, u32[]{:S(2)}) copy-start(f32[8,768]{1,0:T(8,128)} %gc_ref.1) | copy-start | bytes 73732
  4.2 0.7 %copy-start.10 = (f32[8,768]{1,0:T(8,128)S(1)}, f32[8,768]{1,0:T(8,128)}, u32[]{:S(2)}) copy-start(f32[8,768]{1,0:T(8,128)} %gt_ref.1) | copy-start | bytes 73732
  5.0 61.5 %copy-start.2 = (bf16[512,256]{1,0:T(8,128)(2,1)S(1)}, bf16[512,256]{1,0:T(8,128)(2,1)}, u32[]{:S(2)}) copy-start(bf16[512,256]{1,0:T(8,128)(2,1)} %pj_ref.3) | copy-start | bytes 786436
  5.0 61.6 %copy-start.4 = (f32[64,512]{1,0:T(8,128)S(1)}, f32[64,512]{1,0:T(8,128)}, u32[]{:S(2)}) copy-start(f32[64,512]{1,0:T(8,128)} %lm_ref.3) | copy-start | bytes 393220
  5.0 61.6 %copy-start.6 = (f32[64,512]{1,0:T(8,128)S(1)}, f32[64,512]{1,0:T(8,128)}, u32[]{:S(2)}) copy-start(f32[64,512]{1,0:T(8,128)} %ls_ref.3) | copy-start | bytes 393220
  5.0 61.6 %copy-start.7 = (f32[8,2048]{1,0:T(8,128)S(1)}, f32[8,2048]{1,0:T(8,128)}, u32[]{:S(2)}) copy-start(f32[8,2048]{1,0:T(8,128)} %gm_ref.1) | copy-start | bytes 196612
  5.0 61.6 %copy-start.8 = (f32[8,2048]{1,0:T(8,128)S(1)}, f32[8,2048]{1,0:T(8,128)}, u32[]{:S(2)}) copy-start(f32[8,2048]{1,0:T(8,128)} %gq_ref.1) | copy-start | bytes 196612

commit v3 on v2

v3 whole, which is shorter than its diff:
```python
import functools

import jax
import jax.numpy as jnp
from jax import lax
from jax.experimental import pallas as pl
from jax.experimental.pallas import tpu as pltpu
from jax.sharding import PartitionSpec as P

BETA_ONE = 0.9
BETA_TWO = 0.95
STEP_RATE = 0.01
EPSILON = 1e-08
NORM_FLOOR = 1e-06


PIECES = 4
VMEM_GRANT = 32 * 1024 * 1024
MESH = pl.DeviceIdType.MESH
CONTRACT = (((0,), (0,)), ((), ()))


def collective_form(
    attention_input,
    query_cotangent,
    gate_cotangent,
    gate_totals,
    projector,
    query_master,
    lowrank_mean,
    lowrank_square,
    gating_mean,
    gating_square,
):
    tokens_all = attention_input.shape[0] * lax.axis_size("fs") * lax.axis_size("rep")
    norming = 1.0 / tokens_all**0.5
    contract = (((0,), (0,)), ((), ()))
    earlier = jnp.concatenate(
        [jnp.zeros((gate_totals.shape[0], 1), jnp.float32), gate_totals[:, :-1]], axis=1
    )
    gate_logarithm = gate_totals - earlier
    trailing = lax.cumsum(gate_cotangent, axis=1, reverse=True)
    gate_signal = (trailing * -jnp.expm1(gate_logarithm)).astype(jnp.bfloat16)
    gate_partial = jnp.dot(gate_signal, attention_input, preferred_element_type=jnp.float32)
    forget_gradient = lax.psum(gate_partial, ("fs", "rep")) * norming
    thin_rows = lax.psum_scatter(
        lax.dot_general(
            attention_input, query_cotangent, contract, preferred_element_type=jnp.float32
        ),
        ("fs", "rep"),
        scatter_dimension=0,
        tiled=True,
    )
    gradient = lax.all_gather(thin_rows, "rep", axis=0, tiled=True) * norming
    rank_rows = lowrank_mean.shape[0]
    own_factor = lax.dynamic_slice_in_dim(
        projector, lax.axis_index("rep") * rank_rows, rank_rows, 1
    ).astype(jnp.float32)
    rank_partial = lax.dot_general(
        own_factor,
        gradient,
        contract,
        precision=lax.Precision.HIGHEST,
        preferred_element_type=jnp.float32,
    )
    projected = lax.psum(rank_partial, "fs")
    mean_after = BETA_ONE * lowrank_mean + (1.0 - BETA_ONE) * projected
    square_after = BETA_TWO * lowrank_square + (1.0 - BETA_TWO) * projected * projected
    direction = mean_after / (jnp.sqrt(square_after) + EPSILON)
    direction_squares, projected_squares = lax.psum(
        (jnp.sum(direction * direction), jnp.sum(projected * projected)), ("rep", "tp")
    )
    balance = jnp.sqrt(direction_squares / (projected_squares + NORM_FLOOR))
    blended = (direction - balance * projected).astype(jnp.bfloat16)
    lifted = jnp.dot(
        projector,
        lax.all_gather(blended, "rep", axis=0, tiled=True),
        preferred_element_type=jnp.float32,
    )
    query_update = lifted + balance * gradient
    query_renewed = query_master - STEP_RATE * query_update
    query_copy = query_renewed.astype(jnp.bfloat16)
    gating_average = BETA_ONE * gating_mean + (1.0 - BETA_ONE) * forget_gradient
    gating_energy = BETA_TWO * gating_square + (1.0 - BETA_TWO) * forget_gradient * forget_gradient
    gating_update = gating_average / (jnp.sqrt(gating_energy) + EPSILON)
    return (
        query_update,
        query_renewed,
        query_copy,
        mean_after,
        square_after,
        gating_update,
        gating_average,
        gating_energy,
    )


def fused_kernel(
    nf, nr, nt,
    x_hbm, c_hbm, gc_hbm, gt_hbm, pj_hbm, lm_hbm, ls_hbm,
    g_all, h_all, balance_ref, projected_ref, rd_all,
    x_ref, c_ref, gc_ref, gt_ref, lm_ref, ls_ref, p_all,
    a_send, a_recv, a_own, a_keep, m_send, m_recv, b_send, b_recv, g_ref,
    xp_ref, d_part, d_send, d_recv, e_all, f_send, f_recv,
    ra_send, ra_recv, rb_part, rb_recv, rc_all,
    send_sem, recv_sem, load_sem,
):
    f, r, t = lax.axis_index("fs"), lax.axis_index("rep"), lax.axis_index("tp")
    tokens, width = x_ref.shape
    cols = c_ref.shape[1]
    piece = cols // PIECES
    thin = width // (nf * nr)
    half = thin // 2
    rank_rows = lm_ref.shape[0]
    rank_half = p_all.shape[2] // nt
    norming = 1.0 / (tokens * nf * nr) ** 0.5
    fl, bf = jnp.float32, jnp.bfloat16
    started = []
    side, line = lax.rem(r, 2), r // 2
    square = [r, line * 2 + (1 - side), (1 - line) * 2 + side, (1 - line) * 2 + (1 - side)]
    fss, squares = list(range(1, nf)), [1, 2, 3]

    loading = []

    def load(src, dst):
        copy = pltpu.make_async_copy(src, dst, load_sem.at[len(loading)])
        copy.start()
        loading.append(copy)
        return copy

    def columns(owner, j):
        return pl.ds(pl.multiple_of((j * nr + owner) * thin, thin), thin)

    load_c = load(c_hbm, c_ref)
    loads = {}
    for k in [3, 1, 2, 0]:
        for j in range(nf):
            where = columns(square[k], j)
            loads[k, j] = load(x_hbm.at[:, where], x_ref.at[:, where])
        if k == 3:
            load_p = load(pj_hbm, p_all.at[f])
    others = [load(*v) for v in ((gc_hbm, gc_ref), (gt_hbm, gt_ref), (lm_hbm, lm_ref), (ls_hbm, ls_ref))]

    def send(src, dst, where):
        slot = len(started)
        copy = pltpu.make_async_remote_copy(
            src_ref=src, dst_ref=dst, send_sem=send_sem.at[slot], recv_sem=recv_sem.at[slot],
            device_id=where, device_id_type=MESH,
        )
        copy.start()
        started.append(copy)
        return copy

    def rep(k):
        return (f, square[k], t)

    def depth(k):
        return (lax.rem(f + k, nf), r, t)

    rest = [(k, dt) for k in range(4) for dt in range(nt) if k or dt]
    spots = [(f, square[k], lax.rem(t + dt, nt)) for k, dt in rest]
    peers = [depth(k) for k in fss] + spots
    barrier = pltpu.get_barrier_semaphore()
    for peer in peers:
        pl.semaphore_signal(barrier, inc=1, device_id=peer, device_id_type=MESH)

    load_c.wait()

    def block(k, j):
        loads[k, j].wait()
        return lax.dot_general(
            x_ref[:, columns(square[k], j)], c_ref[...], CONTRACT, preferred_element_type=fl
        )

    def cut(p):
        return slice(p * piece, (p + 1) * piece)

    def fill(k, j):
        value = block(k, j)
        upper, lower = value[:half], value[half:]
        if k == 0:
            a_own[j] = value
        if k == 1:
            a_keep[1, j] = lower
        if k == 2:
            a_keep[0, j] = upper
        for h, part, slot in ((0, upper, {3: 0, 1: 1}), (1, lower, {3: 0, 2: 1})):
            if k in slot:
                small = part.astype(bf)
                for p in range(PIECES):
                    a_send[p, h, slot[k], j] = small[:, cut(p)]

    first = {}

    def send_first(p, h, o):
        first[p, h, o] = send(a_send.at[p, h, o], a_recv.at[p, h, o], rep(1 + h))

    second = {}

    def send_second(p):
        for h in range(2):
            first[p, h, 0].wait_recv()
            for j in range(nf):
                value = a_keep[h, j, :, cut(p)] + a_recv[p, h, 0, j].astype(fl)
                m_send[p, h, j] = value.astype(bf)
            second[p, h] = send(m_send.at[p, h], m_recv.at[p, h], rep(2 - h))

    third = {}

    def send_third(p):
        for h in range(2):
            first[p, h, 1].wait_recv()
            second[p, h].wait_recv()

        def summed(h, j):
            rows = slice(h * half, (h + 1) * half)
            return (
                a_own[j, rows, cut(p)] + a_recv[p, h, 1, j].astype(fl)
                + m_recv[p, h, j].astype(fl)
            )

        for k in fss:
            for h in range(2):
                b_send[p, k - 1, h] = summed(h, lax.rem(f + k, nf)).astype(bf)
            third[p, k] = send(b_send.at[p, k - 1], b_recv.at[p, k - 1], depth(k))
        for h in range(2):
            g_ref[h, :, cut(p)] = summed(h, f)

    fourth = []

    def send_fourth(p):
        for k in fss:
            third[p, k].wait_recv()
        for h in range(2):
            total = g_ref[h, :, cut(p)]
            for k in fss:
                total = total + b_recv[p, k - 1, h].astype(fl)
            g_all[r, h * half : (h + 1) * half, cut(p)] = (total * norming).astype(bf)
        where = g_all.at[r, :, cut(p)]
        fourth.extend(send(where, where, rep(k)) for k in squares)

    for j in range(nf):
        fill(3, j)
    load_p.wait()
    pl.semaphore_wait(barrier, len(peers))
    mine = pl.ds(pl.multiple_of(t * rank_half, rank_half), rank_half)
    p_far = [send(p_all.at[f, :, mine], p_all.at[f, :, mine], depth(k)) for k in fss]
    send_first(0, 0, 0)
    send_first(0, 1, 0)
    for k in (1, 2):
        for j in range(nf):
            fill(k, j)
        send_first(0, k - 1, 1)
    for h in range(2):
        for o in range(2):
            send_first(1, h, o)
    for j in range(nf):
        fill(0, j)

    for copy in others:
        copy.wait()
    lanes = 128
    lower = lax.broadcasted_iota(jnp.int32, (lanes, lanes), 0)
    upper = lax.broadcasted_iota(jnp.int32, (lanes, lanes), 1)
    later = (lower >= upper).astype(fl)
    carry = jnp.zeros((gc_ref.shape[0], 1), fl)
    signals = []
    totals = gt_ref[...]
    opens = lax.broadcasted_iota(jnp.int32, totals.shape, 1) == 0
    gate_logarithm = totals - jnp.where(opens, 0.0, pltpu.roll(totals, 1, 1))
    for i in reversed(range(tokens // lanes)):
        window = slice(i * lanes, (i + 1) * lanes)
        own = gc_ref[:, window]
        trailing = carry + jnp.dot(
            own, later, precision=lax.Precision.HIGHEST, preferred_element_type=fl
        )
        carry = carry + jnp.sum(own, axis=1, keepdims=True)
        signals.append(trailing)
    trailing = jnp.concatenate(signals[::-1], axis=1)
    series = jnp.ones_like(gate_logarithm)
    for i in range(8, 1, -1):
        series = 1.0 + gate_logarithm * series / i
    opening = jnp.where(
        gate_logarithm > -0.25, -gate_logarithm * series, 1.0 - jnp.exp(gate_logarithm)
    )
    gate_signal = (trailing * opening).astype(bf)
    gate_partial = jnp.dot(gate_signal, x_ref[...], preferred_element_type=fl)
    for i in range(nr):
        for j in range(nf):
            start = (i * nf + j) * thin
            ra_send[i, j] = gate_partial[:, start : start + thin]
    ra = [send(ra_send.at[square[k]], ra_recv.at[k - 1], rep(k)) for k in squares]

    def cast(q):
        place = lax.rem(f + q, nf)
        where = pl.ds(pl.multiple_of(place * nr * thin, nr * thin), nr * thin)
        return jnp.dot(x_ref[:, where], p_all[place], preferred_element_type=fl)

    xp_ref[...] = cast(0)

    send_second(0)
    for h in range(2):
        for o in range(2):
            send_first(2, h, o)
    send_second(1)

    p_near = []
    for k in fss:
        p_far[k - 1].wait_recv()
        place = lax.rem(f + nf - k, nf)
        where = p_all.at[place, :, mine]
        p_near.append(send(where, where, (f, r, 1 - t)))
    for k in fss:
        p_near[k - 1].wait_recv()
        xp_ref[...] += cast(nf - k)
    cast_all = xp_ref[...]
    high = cast_all.astype(bf)
    low = (cast_all - high.astype(fl)).astype(bf)
    partial = lax.dot_general(high, c_ref[...], CONTRACT, preferred_element_type=fl)
    partial += lax.dot_general(low, c_ref[...], CONTRACT, preferred_element_type=fl)
    d_part[...] = (partial * norming).reshape(d_part.shape)
    d = []
    for k in squares:
        d_send[k - 1] = d_part[square[k]].astype(bf)
        d.append(send(d_send.at[k - 1], d_recv.at[k - 1], rep(k)))
    for h in range(2):
        for o in range(2):
            send_first(3, h, o)
    send_third(0)
    send_second(2)
    send_third(1)

    for copy in d:
        copy.wait_recv()
    total = d_part[r]
    for k in squares:
        total = total + d_recv[k - 1].astype(fl)
    e_all[f] = total.astype(bf)
    e = [send(e_all.at[f], e_all.at[f], depth(k)) for k in fss]

    for copy in ra:
        copy.wait_recv()
    gate_rows = ra_send[r]
    for k in squares:
        gate_rows = gate_rows + ra_recv[k - 1]
    rb_part[...] = gate_rows
    rb = [send(rb_part.at[lax.rem(f + k, nf)], rb_recv.at[k - 1], depth(k)) for k in fss]

    send_second(3)
    send_third(2)
    send_fourth(0)
    send_fourth(1)
    for copy in rb:
        copy.wait_recv()
    gate_block = rb_part[f]
    for k in fss:
        gate_block = gate_block + rb_recv[k - 1]
    rc_all[f] = gate_block * norming
    rc = [send(rc_all.at[f], rc_all.at[f], depth(k)) for k in fss]
    send_third(3)

    for copy in e:
        copy.wait_recv()
    projected = e_all[0].astype(fl)
    for j in fss:
        projected = projected + e_all[j].astype(fl)
    mean_after = BETA_ONE * lm_ref[...] + (1.0 - BETA_ONE) * projected
    square_after = BETA_TWO * ls_ref[...] + (1.0 - BETA_TWO) * projected * projected
    direction = mean_after / (jnp.sqrt(square_after) + EPSILON)
    top = lax.broadcasted_iota(jnp.int32, f_send.shape, 0) == 0
    f_send[...] = jnp.where(top, jnp.sum(direction * direction), jnp.sum(projected * projected))
    fc = [send(f_send, f_recv.at[i], spot) for i, spot in enumerate(spots)]
    projected_ref[...] = projected
    send_fourth(2)
    for copy in fc:
        copy.wait_recv()
    sums = f_send[...]
    for i in range(len(rest)):
        sums = sums + f_recv[i]
    balance = jnp.sqrt(sums[:1, :1] / (sums[1:2, :1] + NORM_FLOOR))
    balance_ref[...] = jnp.broadcast_to(balance, balance_ref.shape)
    h_all[r] = (direction - balance * projected).astype(bf)
    hs = [send(h_all.at[r], h_all.at[r], rep(k)) for k in squares]

    for copy in rc:
        copy.wait_recv()
    rd_all[r] = rc_all[...]
    rd = [send(rd_all.at[r], rd_all.at[r], rep(k)) for k in squares]
    send_fourth(3)
    for copy in rd + hs + fourth:
        copy.wait_recv()
    for copy in started:
        copy.wait_send()


def closing_kernel(
    g_ref, h_ref, balance_ref, projected_ref, gate_ref, pj_ref, qm_ref, lm_ref, ls_ref, gm_ref, gq_ref,
    qu_ref, qr_ref, qc_ref, ma_ref, sa_ref, gu_ref, ga_ref, ge_ref,
):
    lifted = jnp.dot(
        pj_ref[...], h_ref[...].reshape(pj_ref.shape[1], qm_ref.shape[1]),
        preferred_element_type=jnp.float32,
    )
    query_update = lifted + balance_ref[:1, :1] * g_ref[0].astype(jnp.float32)
    query_renewed = qm_ref[...] - STEP_RATE * query_update
    qu_ref[...] = query_update
    qr_ref[...] = query_renewed
    qc_ref[...] = query_renewed.astype(jnp.bfloat16)

    @pl.when(pl.program_id(0) == 0)
    def _():
        projected = projected_ref[...]
        ma_ref[...] = BETA_ONE * lm_ref[...] + (1.0 - BETA_ONE) * projected
        sa_ref[...] = BETA_TWO * ls_ref[...] + (1.0 - BETA_TWO) * projected * projected
        nr, nf, _, thin = gate_ref.shape
        for i in range(nr):
            for j in range(nf):
                window = slice((i * nf + j) * thin, (i * nf + j + 1) * thin)
                forget_gradient = gate_ref[i, j]
                average = BETA_ONE * gm_ref[:, window] + (1.0 - BETA_ONE) * forget_gradient
                energy = (
                    BETA_TWO * gq_ref[:, window]
                    + (1.0 - BETA_TWO) * forget_gradient * forget_gradient
                )
                ga_ref[:, window] = average
                ge_ref[:, window] = energy
                gu_ref[:, window] = average / (jnp.sqrt(energy) + EPSILON)


def per_device(nf, nr, nt, *args):
    x, c, gc, gt, pj, qm, lm, ls, gm, gq = args
    width, cols, rank_rows, heads = x.shape[1], c.shape[1], lm.shape[0], gc.shape[0]
    thin = width // (nf * nr)
    fits = (
        width % (nf * nr * 128) == 0 and rank_rows % 16 == 0
        and cols % (PIECES * 128) == 0 and heads % 8 == 0 and nf > 1 and nr == 4 and nt == 2
        and x.shape[0] % 128 == 0 and pj.shape[1] % (nt * 128) == 0
    )
    if not fits:
        return collective_form(*args)
    piece, half, bf, fl = cols // PIECES, thin // 2, jnp.bfloat16, jnp.float32
    rank_all = pj.shape[1]
    scratch = [
        (x.shape, bf), (c.shape, bf), (gc.shape, fl), (gt.shape, fl), (lm.shape, fl),
        (ls.shape, fl), ((nf, nr * thin, rank_all), bf),
        ((PIECES, 2, 2, nf, half, piece), bf), ((PIECES, 2, 2, nf, half, piece), bf),
        ((nf, thin, cols), fl), ((2, nf, half, cols), fl),
        ((PIECES, 2, nf, half, piece), bf), ((PIECES, 2, nf, half, piece), bf),
        ((PIECES, nf - 1, 2, half, piece), bf), ((PIECES, nf - 1, 2, half, piece), bf),
        ((2, half, cols), fl),
        ((x.shape[0], rank_all), fl), ((nr, rank_rows, cols), fl),
        ((nr - 1, rank_rows, cols), bf), ((nr - 1, rank_rows, cols), bf),
        ((nf, rank_rows, cols), bf), ((8, 128), fl), ((nr * nt - 1, 8, 128), fl),
        ((nr, nf, heads, thin), fl), ((nr - 1, nf, heads, thin), fl),
        ((nf, heads, thin), fl), ((nf - 1, heads, thin), fl),
        ((nf, heads, thin), fl),
    ]
    copies = PIECES * 6 + (PIECES + 4) * (nr - 1) + (PIECES + 5) * (nf - 1) + nr * nt - 1
    outs = [
        (qm.shape, fl), (qm.shape, fl), (qm.shape, bf), (lm.shape, fl), (lm.shape, fl),
        (gm.shape, fl), (gm.shape, fl), (gm.shape, fl),
    ]
    between = [
        ((nr, thin, cols), bf), ((nr, rank_rows, cols), bf), ((8, 128), fl), (lm.shape, fl),
        ((nr, nf, heads, thin), fl),
    ]
    vmem = pl.BlockSpec(memory_space=pltpu.VMEM)
    hbm = pl.BlockSpec(memory_space=pltpu.HBM)
    passed = pl.pallas_call(
        functools.partial(fused_kernel, nf, nr, nt),
        out_shape=tuple(jax.ShapeDtypeStruct(*o) for o in between),
        in_specs=[hbm] * 7,
        out_specs=(vmem,) * len(between),
        scratch_shapes=[pltpu.VMEM(*v) for v in scratch]
        + [pltpu.SemaphoreType.DMA((copies,)), pltpu.SemaphoreType.DMA((copies,))]
        + [pltpu.SemaphoreType.DMA((nr * nf + 6,))],
        compiler_params=pltpu.CompilerParams(
            collective_id=0, has_side_effects=True, vmem_limit_bytes=VMEM_GRANT
        ),
    )(*(pltpu.with_memory_space_constraint(v, pltpu.HBM) for v in (x, c, gc, gt, pj, lm, ls)))

    def whole(shape):
        return pl.BlockSpec(shape, lambda i: (0,) * len(shape))

    def rows(width):
        return pl.BlockSpec((thin, width), lambda i: (i, 0))

    return pl.pallas_call(
        closing_kernel,
        grid=(nr,),
        out_shape=tuple(jax.ShapeDtypeStruct(*o) for o in outs),
        in_specs=[pl.BlockSpec((1, thin, cols), lambda i: (i, 0, 0))]
        + [whole(b[0]) for b in between[1:]]
        + [rows(pj.shape[1]), rows(cols), whole(lm.shape), whole(ls.shape)]
        + [whole(gm.shape), whole(gq.shape)],
        out_specs=(rows(cols),) * 3 + tuple(whole(o[0]) for o in outs[3:]),
        compiler_params=pltpu.CompilerParams(vmem_limit_bytes=VMEM_GRANT),
    )(*passed, pj, qm, lm, ls, gm, gq)


def solution(mesh):
    in_specs = (
        P(("fs", "rep"), None),
        P(("fs", "rep"), "tp"),
        P("tp", ("fs", "rep")),
        P("tp", ("fs", "rep")),
        P("fs", None),
        P("fs", "tp"),
        P("rep", "tp"),
        P("rep", "tp"),
        P("tp", None),
        P("tp", None),
    )
    out_specs = (
        P("fs", "tp"),
        P("fs", "tp"),
        P("fs", "tp"),
        P("rep", "tp"),
        P("rep", "tp"),
        P("tp", None),
        P("tp", None),
        P("tp", None),
    )
    return jax.shard_map(
        functools.partial(per_device, mesh.shape["fs"], mesh.shape["rep"], mesh.shape["tp"]),
        mesh=mesh, in_specs=in_specs, out_specs=out_specs, check_vma=False
    )
```

time: 69.5 us -> 51.2 us (0.74)
  Pallas kernels: 64.1 us -> 50.2 us
  local copies, waits for them, and re-layouts: 4.33 us -> 0.03 us
    pallas_call x1, Pallas kernels: 61.5 us -> 47.6 us  [per_device(): pl.pallas_call(functools.partial(fused_kernel, nf, nr, nt), out_shape=tup...]
    unnamed x22 -> x12, local copies, waits for them, and re-layouts: 4.33 us -> 0.03 us
where the time goes in v3:
time: 51.2 us; the launch traced here: 51 us
  Pallas kernels  50.2 us (98%)
  between operations  0.74 us (1%)
    pallas_call x1, Pallas kernels, per_device(): pl.pallas_call(functools.partial(fused_kernel, nf, nr, nt), out_shape=tup...  47.6 us
    pallas_call x1, Pallas kernels, per_device(): pl.pallas_call(closing_kernel, grid=(nr,), out_shape=tuple((jax.ShapeDtyp...  2.64 us

profile of v3, /device:TPU:0, one launch (start us, length us, event | category | flops | bytes accessed | tf_op | source)
XLA Modules:
  0.0 51.0 jit_solution(6181382670178529878)
XLA Ops:
  0.6 0.0 copy-start.3
  0.6 0.0 copy-start.2
  0.7 0.0 copy-start.1
  0.7 0.0 copy-start.5
  0.7 0.0 copy-start.4
  0.7 0.0 copy-start
  0.7 47.6 %shard_map.161 = (bf16[4,128,512]{2,1,0:T(8,128)(2,1)S(1)}, bf16[4,64,512]{2,1,0:T(8,128)(2,1)S(1)}, f32[8,128]{1,0:T(8,128)S(1)}, f32[64,512]{1,0:T(8,128)S(1)}, f32[4,4,8,128]{3,2,1,0:T(8,128)S(1)}) custom-call(bf16[768,2048]{1,0:T(8,128)(2,1)} %x_hbm.1, bf16[768,512]{1,0:T(8,128)(2,1)} %c_hbm.1, f32[8,768]{1,0:T(8,128)} %gc_hbm.1, f32[8,768]{1,0:T(8,128)} %gt_hbm.1, ...), custom_call_target="tpu_custom_call" | custom-call | tf_op jit(solution)/shard_map/pallas_call | solution.py:469
  48.3 0.0 copy-done.3
  48.3 0.0 copy-done.2
  48.3 0.0 copy-done.1
  48.3 0.0 copy-done.5
  48.3 0.0 copy-done.4
  48.4 0.0 copy-done
  48.4 2.6 %shard_map.162 = (f32[512,512]{1,0:T(8,128)}, f32[512,512]{1,0:T(8,128)}, bf16[512,512]{1,0:T(8,128)(2,1)}, f32[64,512]{1,0:T(8,128)}, f32[64,512]{1,0:T(8,128)}...) custom-call(bf16[4,128,512]{2,1,0:T(8,128)(2,1)S(1)} %get-tuple-element.13.g_ref, ...), custom_call_target="tpu_custom_call" | custom-call | tf_op jit(solution)/shard_map/pallas_call | solution.py:488
Async XLA Ops:
  0.6 47.7 %copy-start.3 = (f32[64,512]{1,0:T(8,128)S(1)}, f32[64,512]{1,0:T(8,128)}, u32[]{:S(2)}) copy-start(f32[64,512]{1,0:T(8,128)} %ls_ref.1) | copy-start | bytes 393220
  0.6 47.7 %copy-start.2 = (f32[64,512]{1,0:T(8,128)S(1)}, f32[64,512]{1,0:T(8,128)}, u32[]{:S(2)}) copy-start(f32[64,512]{1,0:T(8,128)} %lm_ref.1) | copy-start | bytes 393220
  0.7 47.7 %copy-start.1 = (bf16[512,256]{1,0:T(8,128)(2,1)S(1)}, bf16[512,256]{1,0:T(8,128)(2,1)}, u32[]{:S(2)}) copy-start(bf16[512,256]{1,0:T(8,128)(2,1)} %pj_ref.1) | copy-start | bytes 786436
  0.7 47.7 %copy-start.5 = (f32[8,2048]{1,0:T(8,128)S(1)}, f32[8,2048]{1,0:T(8,128)}, u32[]{:S(2)}) copy-start(f32[8,2048]{1,0:T(8,128)} %gq_ref.1) | copy-start | bytes 196612
  0.7 47.7 %copy-start.4 = (f32[8,2048]{1,0:T(8,128)S(1)}, f32[8,2048]{1,0:T(8,128)}, u32[]{:S(2)}) copy-start(f32[8,2048]{1,0:T(8,128)} %gm_ref.1) | copy-start | bytes 196612
  0.7 47.7 %copy-start = (f32[512,512]{1,0:T(8,128)S(1)}, f32[512,512]{1,0:T(8,128)}, u32[]{:S(2)}) copy-start(f32[512,512]{1,0:T(8,128)} %qm_ref.1) | copy-start | bytes 3145732

commit v4 on v3

--- a/solution.py
+++ b/solution.py
@@ -99,9 +99,9 @@
     nf, nr, nt,
     x_hbm, c_hbm, gc_hbm, gt_hbm, pj_hbm, lm_hbm, ls_hbm,
     g_all, h_all, balance_ref, projected_ref, rd_all,
-    x_ref, c_ref, gc_ref, gt_ref, lm_ref, ls_ref, p_all,
+    x_ref, c_ref, c_twin, gc_ref, gt_ref, lm_ref, ls_ref, p_all,
     a_send, a_recv, a_own, a_keep, m_send, m_recv, b_send, b_recv, g_ref,
-    xp_ref, d_part, d_send, d_recv, e_all, f_send, f_recv,
+    xp_ref, d_send, d_recv, e_all, f_send, f_recv,
     ra_send, ra_recv, rb_part, rb_recv, rc_all,
     send_sem, recv_sem, load_sem,
 ):
@@ -112,44 +112,45 @@
     thin = width // (nf * nr)
     half = thin // 2
     rank_rows = lm_ref.shape[0]
-    rank_half = p_all.shape[2] // nt
+    rank_half = p_all.shape[2]
     norming = 1.0 / (tokens * nf * nr) ** 0.5
     fl, bf = jnp.float32, jnp.bfloat16
-    started = []
     side, line = lax.rem(r, 2), r // 2
     square = [r, line * 2 + (1 - side), (1 - line) * 2 + side, (1 - line) * 2 + (1 - side)]
     fss, squares = list(range(1, nf)), [1, 2, 3]
 
-    loading = []
-
-    def load(src, dst):
-        copy = pltpu.make_async_copy(src, dst, load_sem.at[len(loading)])
-        copy.start()
-        loading.append(copy)
-        return copy
-
     def columns(owner, j):
         return pl.ds(pl.multiple_of((j * nr + owner) * thin, thin), thin)
 
-    load_c = load(c_hbm, c_ref)
-    loads = {}
+    def load(slot, src, dst):
+        pltpu.make_async_copy(src, dst, load_sem.at[slot]).start()
+
+    def settle(sem, ref):
+        pltpu.make_async_copy(ref, ref, sem).wait()
+
+    mine = pl.ds(pl.multiple_of(t * rank_half, rank_half), rank_half)
+    load(nr, c_hbm, c_ref)
+    load(nr + 1, pj_hbm.at[:, mine], p_all.at[f])
     for k in [3, 1, 2, 0]:
         for j in range(nf):
             where = columns(square[k], j)
-            loads[k, j] = load(x_hbm.at[:, where], x_ref.at[:, where])
-        if k == 3:
-            load_p = load(pj_hbm, p_all.at[f])
-    others = [load(*v) for v in ((gc_hbm, gc_ref), (gt_hbm, gt_ref), (lm_hbm, lm_ref), (ls_hbm, ls_ref))]
-
-    def send(src, dst, where):
-        slot = len(started)
+            load(k, x_hbm.at[:, where], x_ref.at[:, where])
+    for i, v in enumerate(((gc_hbm, gc_ref), (gt_hbm, gt_ref), (lm_hbm, lm_ref), (ls_hbm, ls_ref))):
+        load(nr + 2 + i, *v)
+
+    groups, arrivals, totals_sent = {}, {}, {}
+
+    def send(group, key, src, dst, where):
         copy = pltpu.make_async_remote_copy(
-            src_ref=src, dst_ref=dst, send_sem=send_sem.at[slot], recv_sem=recv_sem.at[slot],
+            src_ref=src, dst_ref=dst,
+            send_sem=send_sem.at[groups.setdefault(group, len(groups))],
+            recv_sem=recv_sem.at[arrivals.setdefault(key, len(arrivals))],
             device_id=where, device_id_type=MESH,
         )
         copy.start()
-        started.append(copy)
-        return copy
+
+    def arrive(key, ref):
+        settle(recv_sem.at[arrivals[key]], ref)
 
     def rep(k):
         return (f, square[k], t)
@@ -157,26 +158,21 @@
     def depth(k):
         return (lax.rem(f + k, nf), r, t)
 
-    rest = [(k, dt) for k in range(4) for dt in range(nt) if k or dt]
-    spots = [(f, square[k], lax.rem(t + dt, nt)) for k, dt in rest]
+    spots = [(f, square[k], lax.rem(t + dt, nt)) for k in range(4) for dt in range(nt) if k or dt]
     peers = [depth(k) for k in fss] + spots
     barrier = pltpu.get_barrier_semaphore()
     for peer in peers:
         pl.semaphore_signal(barrier, inc=1, device_id=peer, device_id_type=MESH)
 
-    load_c.wait()
-
-    def block(k, j):
-        loads[k, j].wait()
-        return lax.dot_general(
+    settle(load_sem.at[nr], c_ref)
+
+    def cut(p):
+        return slice(p * piece, (p + 1) * piece)
+
+    def fill(k, j):
+        value = lax.dot_general(
             x_ref[:, columns(square[k], j)], c_ref[...], CONTRACT, preferred_element_type=fl
         )
-
-    def cut(p):
-        return slice(p * piece, (p + 1) * piece)
-
-    def fill(k, j):
-        value = block(k, j)
         upper, lower = value[:half], value[half:]
         if k == 0:
             a_own[j] = value
@@ -190,27 +186,31 @@
                 for p in range(PIECES):
                     a_send[p, h, slot[k], j] = small[:, cut(p)]
 
-    first = {}
-
-    def send_first(p, h, o):
-        first[p, h, o] = send(a_send.at[p, h, o], a_recv.at[p, h, o], rep(1 + h))
-
-    second = {}
+    def ready(k):
+        settle(load_sem.at[k], x_ref.at[:, : nf * thin])
+
+    def send_open(h, o):
+        send("first", ("open", o), a_send.at[0, h, o], a_recv.at[0, h, o], rep(1 + h))
+
+    def send_first(p):
+        for h in range(2):
+            send("first", ("first", p), a_send.at[p, h], a_recv.at[p, h], rep(1 + h))
 
     def send_second(p):
+        if p == 0:
+            arrive(("open", 0), a_recv.at[0, :, 0])
+        else:
+            arrive(("first", p), a_recv.at[p])
         for h in range(2):
-            first[p, h, 0].wait_recv()
             for j in range(nf):
                 value = a_keep[h, j, :, cut(p)] + a_recv[p, h, 0, j].astype(fl)
                 m_send[p, h, j] = value.astype(bf)
-            second[p, h] = send(m_send.at[p, h], m_recv.at[p, h], rep(2 - h))
-
-    third = {}
+            send("second", ("second", p), m_send.at[p, h], m_recv.at[p, h], rep(2 - h))
 
     def send_third(p):
-        for h in range(2):
-            first[p, h, 1].wait_recv()
-            second[p, h].wait_recv()
+        if p == 0:
+            arrive(("open", 1), a_recv.at[0, :, 1])
+        arrive(("second", p), m_recv.at[p])
 
         def summed(h, j):
             rows = slice(h * half, (h + 1) * half)
@@ -222,43 +222,54 @@
         for k in fss:
             for h in range(2):
                 b_send[p, k - 1, h] = summed(h, lax.rem(f + k, nf)).astype(bf)
-            third[p, k] = send(b_send.at[p, k - 1], b_recv.at[p, k - 1], depth(k))
+            send("third", ("third", p), b_send.at[p, k - 1], b_recv.at[p, k - 1], depth(k))
         for h in range(2):
             g_ref[h, :, cut(p)] = summed(h, f)
 
-    fourth = []
-
     def send_fourth(p):
-        for k in fss:
-            third[p, k].wait_recv()
+        arrive(("third", p), b_recv.at[p])
         for h in range(2):
             total = g_ref[h, :, cut(p)]
             for k in fss:
                 total = total + b_recv[p, k - 1, h].astype(fl)
             g_all[r, h * half : (h + 1) * half, cut(p)] = (total * norming).astype(bf)
         where = g_all.at[r, :, cut(p)]
-        fourth.extend(send(where, where, rep(k)) for k in squares)
-
-    for j in range(nf):
+        for k in squares:
+            send("fourth", "fourth", where, where, rep(k))
+
+    ready(3)
+    fill(3, 0)
+    fill(3, 1)
+    settle(load_sem.at[nr + 1], p_all.at[0])
+    pl.semaphore_wait(barrier, len(peers))
+    for k in fss:
+        send("cast", ("cast", k), p_all.at[f], p_all.at[f], depth(k))
+    send("twin", "twin", c_ref, c_twin, (f, r, 1 - t))
+    for j in range(2, nf):
         fill(3, j)
-    load_p.wait()
-    pl.semaphore_wait(barrier, len(peers))
-    mine = pl.ds(pl.multiple_of(t * rank_half, rank_half), rank_half)
-    p_far = [send(p_all.at[f, :, mine], p_all.at[f, :, mine], depth(k)) for k in fss]
-    send_first(0, 0, 0)
-    send_first(0, 1, 0)
+    send_open(0, 0)
+    send_open(1, 0)
     for k in (1, 2):
+        ready(k)
         for j in range(nf):
             fill(k, j)
-        send_first(0, k - 1, 1)
-    for h in range(2):
-        for o in range(2):
-            send_first(1, h, o)
+        send_open(k - 1, 1)
+    send_first(1)
+    ready(0)
     for j in range(nf):
         fill(0, j)
-
-    for copy in others:
-        copy.wait()
+    send_second(0)
+    send_first(2)
+
+    def cast(q):
+        place = lax.rem(f + q, nf)
+        where = pl.ds(pl.multiple_of(place * nr * thin, nr * thin), nr * thin)
+        return jnp.dot(x_ref[:, where], p_all[place], preferred_element_type=fl)
+
+    xp_ref[...] = cast(0)
+
+    for i, ref in enumerate((gc_ref, gt_ref, lm_ref, ls_ref)):
+        settle(load_sem.at[nr + 2 + i], ref)
     lanes = 128
     lower = lax.broadcasted_iota(jnp.int32, (lanes, lanes), 0)
     upper = lax.broadcasted_iota(jnp.int32, (lanes, lanes), 1)
@@ -289,78 +300,82 @@
         for j in range(nf):
             start = (i * nf + j) * thin
             ra_send[i, j] = gate_partial[:, start : start + thin]
-    ra = [send(ra_send.at[square[k]], ra_recv.at[k - 1], rep(k)) for k in squares]
-
-    def cast(q):
-        place = lax.rem(f + q, nf)
-        where = pl.ds(pl.multiple_of(place * nr * thin, nr * thin), nr * thin)
-        return jnp.dot(x_ref[:, where], p_all[place], preferred_element_type=fl)
-
-    xp_ref[...] = cast(0)
-
-    send_second(0)
-    for h in range(2):
-        for o in range(2):
-            send_first(2, h, o)
+    for k in squares:
+        send("ra", "ra", ra_send.at[square[k]], ra_recv.at[k - 1], rep(k))
+
+    for k in fss[:-1]:
+        arrive(("cast", k), p_all.at[0])
+        xp_ref[...] += cast(nf - k)
     send_second(1)
-
-    p_near = []
-    for k in fss:
-        p_far[k - 1].wait_recv()
-        place = lax.rem(f + nf - k, nf)
-        where = p_all.at[place, :, mine]
-        p_near.append(send(where, where, (f, r, 1 - t)))
-    for k in fss:
-        p_near[k - 1].wait_recv()
-        xp_ref[...] += cast(nf - k)
-    cast_all = xp_ref[...]
+    arrive(("cast", nf - 1), p_all.at[0])
+    cast_all = xp_ref[...] + cast(1)
     high = cast_all.astype(bf)
     low = (cast_all - high.astype(fl)).astype(bf)
-    partial = lax.dot_general(high, c_ref[...], CONTRACT, preferred_element_type=fl)
-    partial += lax.dot_general(low, c_ref[...], CONTRACT, preferred_element_type=fl)
-    d_part[...] = (partial * norming).reshape(d_part.shape)
-    d = []
+    arrive("twin", c_twin)
+    crossed = lax.rem(line + t, 2)
+    for u, ref in ((1, c_twin), (0, c_ref)):
+        partial = lax.dot_general(high, ref[...], CONTRACT, preferred_element_type=fl)
+        partial += lax.dot_general(low, ref[...], CONTRACT, preferred_element_type=fl)
+        partial = (partial * norming).astype(bf)
+        straight, across = partial[:rank_rows], partial[rank_rows:]
+        d_send[0, u] = jnp.where(side == 0, straight, across)
+        d_send[1, u] = jnp.where(side == 0, across, straight)
+        core = lax.rem(t + u, nt)
+        near = (f, (1 - crossed) * square[0] + crossed * square[2], core)
+        far = (f, (1 - crossed) * square[1] + crossed * square[3], core)
+        send("d", "d", d_send.at[1, u], d_recv.at[1 + 2 * crossed], far)
+        if u == 1:
+            send("d", "d", d_send.at[0, u], d_recv.at[2 * crossed], near)
+        else:
+            @pl.when(crossed == 0)
+            def _():
+                d_recv[0] = d_send[0, 0]
+
+            @pl.when(crossed == 1)
+            def _():
+                send("d1", "d", d_send.at[0, 0], d_recv.at[2], rep(2))
+
+    send_second(2)
+    send_first(3)
+    send_third(0)
+    send_third(1)
+
+    @pl.when(crossed == 0)
+    def _():
+        arrive("d", d_recv.at[: nr - 1])
+
+    @pl.when(crossed == 1)
+    def _():
+        arrive("d", d_recv)
+
+    total = d_recv[0].astype(fl)
     for k in squares:
-        d_send[k - 1] = d_part[square[k]].astype(bf)
-        d.append(send(d_send.at[k - 1], d_recv.at[k - 1], rep(k)))
-    for h in range(2):
-        for o in range(2):
-            send_first(3, h, o)
-    send_third(0)
-    send_second(2)
-    send_third(1)
-
-    for copy in d:
-        copy.wait_recv()
-    total = d_part[r]
-    for k in squares:
-        total = total + d_recv[k - 1].astype(fl)
+        total = total + d_recv[k].astype(fl)
     e_all[f] = total.astype(bf)
-    e = [send(e_all.at[f], e_all.at[f], depth(k)) for k in fss]
-
-    for copy in ra:
-        copy.wait_recv()
+    for k in fss:
+        send("e", "e", e_all.at[f], e_all.at[f], depth(k))
+
+    arrive("ra", ra_recv)
     gate_rows = ra_send[r]
     for k in squares:
         gate_rows = gate_rows + ra_recv[k - 1]
     rb_part[...] = gate_rows
-    rb = [send(rb_part.at[lax.rem(f + k, nf)], rb_recv.at[k - 1], depth(k)) for k in fss]
-
+    for k in fss:
+        send("rb", "rb", rb_part.at[lax.rem(f + k, nf)], rb_recv.at[k - 1], depth(k))
+
+    send_fourth(0)
+    send_third(2)
     send_second(3)
-    send_third(2)
-    send_fourth(0)
     send_fourth(1)
-    for copy in rb:
-        copy.wait_recv()
+    arrive("rb", rb_recv)
     gate_block = rb_part[f]
     for k in fss:
         gate_block = gate_block + rb_recv[k - 1]
     rc_all[f] = gate_block * norming
-    rc = [send(rc_all.at[f], rc_all.at[f], depth(k)) for k in fss]
-    send_third(3)
-
-    for copy in e:
-        copy.wait_recv()
+    for k in fss:
+        send("rc", "rc", rc_all.at[f], rc_all.at[f], depth(k))
+
+    arrive("e", e_all.at[: nf - 1])
     projected = e_all[0].astype(fl)
     for j in fss:
         projected = projected + e_all[j].astype(fl)
@@ -369,28 +384,41 @@
     direction = mean_after / (jnp.sqrt(square_after) + EPSILON)
     top = lax.broadcasted_iota(jnp.int32, f_send.shape, 0) == 0
     f_send[...] = jnp.where(top, jnp.sum(direction * direction), jnp.sum(projected * projected))
-    fc = [send(f_send, f_recv.at[i], spot) for i, spot in enumerate(spots)]
+    for i, spot in enumerate(spots):
+        send("f", "f", f_send, f_recv.at[i], spot)
     projected_ref[...] = projected
-    send_fourth(2)
-    for copy in fc:
-        copy.wait_recv()
+    send_third(3)
+    arrive("f", f_recv)
     sums = f_send[...]
-    for i in range(len(rest)):
+    for i in range(len(spots)):
         sums = sums + f_recv[i]
     balance = jnp.sqrt(sums[:1, :1] / (sums[1:2, :1] + NORM_FLOOR))
     balance_ref[...] = jnp.broadcast_to(balance, balance_ref.shape)
     h_all[r] = (direction - balance * projected).astype(bf)
-    hs = [send(h_all.at[r], h_all.at[r], rep(k)) for k in squares]
-
-    for copy in rc:
-        copy.wait_recv()
+    for k in squares:
+        send("h", "h", h_all.at[r], h_all.at[r], rep(k))
+
+    send_fourth(2)
+    arrive("rc", rc_all.at[: nf - 1])
     rd_all[r] = rc_all[...]
-    rd = [send(rd_all.at[r], rd_all.at[r], rep(k)) for k in squares]
+    for k in squares:
+        send("rd", "rd", rd_all.at[r], rd_all.at[r], rep(k))
     send_fourth(3)
-    for copy in rd + hs + fourth:
-        copy.wait_recv()
-    for copy in started:
-        copy.wait_send()
+    arrive("rd", rd_all.at[: nr - 1])
+    arrive("h", h_all.at[: nr - 1])
+    arrive("fourth", g_all.at[: nr - 1])
+    sent = {
+        "first": a_send, "cast": p_all.at[: nf - 1], "twin": c_ref, "second": m_send,
+        "third": b_send, "fourth": g_all.at[: nr - 1], "d": d_recv.at[: nr - 1],
+        "e": e_all.at[: nf - 1], "f": f_recv, "h": h_all.at[: nr - 1], "ra": ra_recv,
+        "rb": rb_recv, "rc": rc_all.at[: nf - 1], "rd": rd_all.at[: nr - 1],
+    }
+    for group, ref in sent.items():
+        settle(send_sem.at[groups[group]], ref)
+
+    @pl.when(crossed == 1)
+    def _():
+        settle(send_sem.at[groups["d1"]], d_send.at[0, 0])
 
 
 def closing_kernel(
@@ -430,32 +458,31 @@
 def per_device(nf, nr, nt, *args):
     x, c, gc, gt, pj, qm, lm, ls, gm, gq = args
     width, cols, rank_rows, heads = x.shape[1], c.shape[1], lm.shape[0], gc.shape[0]
+    rank_all = pj.shape[1]
     thin = width // (nf * nr)
     fits = (
         width % (nf * nr * 128) == 0 and rank_rows % 16 == 0
         and cols % (PIECES * 128) == 0 and heads % 8 == 0 and nf > 1 and nr == 4 and nt == 2
-        and x.shape[0] % 128 == 0 and pj.shape[1] % (nt * 128) == 0
+        and x.shape[0] % 128 == 0 and rank_all % (nt * 128) == 0
     )
     if not fits:
         return collective_form(*args)
     piece, half, bf, fl = cols // PIECES, thin // 2, jnp.bfloat16, jnp.float32
-    rank_all = pj.shape[1]
     scratch = [
-        (x.shape, bf), (c.shape, bf), (gc.shape, fl), (gt.shape, fl), (lm.shape, fl),
-        (ls.shape, fl), ((nf, nr * thin, rank_all), bf),
+        (x.shape, bf), (c.shape, bf), (c.shape, bf), (gc.shape, fl), (gt.shape, fl),
+        (lm.shape, fl), (ls.shape, fl), ((nf, nr * thin, rank_all // nt), bf),
         ((PIECES, 2, 2, nf, half, piece), bf), ((PIECES, 2, 2, nf, half, piece), bf),
         ((nf, thin, cols), fl), ((2, nf, half, cols), fl),
         ((PIECES, 2, nf, half, piece), bf), ((PIECES, 2, nf, half, piece), bf),
         ((PIECES, nf - 1, 2, half, piece), bf), ((PIECES, nf - 1, 2, half, piece), bf),
         ((2, half, cols), fl),
-        ((x.shape[0], rank_all), fl), ((nr, rank_rows, cols), fl),
-        ((nr - 1, rank_rows, cols), bf), ((nr - 1, rank_rows, cols), bf),
+        ((x.shape[0], rank_all // nt), fl),
+        ((2, nt, rank_rows, cols), bf), ((nr, rank_rows, cols), bf),
         ((nf, rank_rows, cols), bf), ((8, 128), fl), ((nr * nt - 1, 8, 128), fl),
         ((nr, nf, heads, thin), fl), ((nr - 1, nf, heads, thin), fl),
         ((nf, heads, thin), fl), ((nf - 1, heads, thin), fl),
         ((nf, heads, thin), fl),
     ]
-    copies = PIECES * 6 + (PIECES + 4) * (nr - 1) + (PIECES + 5) * (nf - 1) + nr * nt - 1
     outs = [
         (qm.shape, fl), (qm.shape, fl), (qm.shape, bf), (lm.shape, fl), (lm.shape, fl),
         (gm.shape, fl), (gm.shape, fl), (gm.shape, fl),
@@ -466,14 +493,14 @@
     ]
     vmem = pl.BlockSpec(memory_space=pltpu.VMEM)
     hbm = pl.BlockSpec(memory_space=pltpu.HBM)
+    semaphores = (15, 3 * PIECES + nf + 10, nr + 6)
     passed = pl.pallas_call(
         functools.partial(fused_kernel, nf, nr, nt),
         out_shape=tuple(jax.ShapeDtypeStruct(*o) for o in between),
         in_specs=[hbm] * 7,
         out_specs=(vmem,) * len(between),
         scratch_shapes=[pltpu.VMEM(*v) for v in scratch]
-        + [pltpu.SemaphoreType.DMA((copies,)), pltpu.SemaphoreType.DMA((copies,))]
-        + [pltpu.SemaphoreType.DMA((nr * nf + 6,))],
+        + [pltpu.SemaphoreType.DMA((n,)) for n in semaphores],
         compiler_params=pltpu.CompilerParams(
             collective_id=0, has_side_effects=True, vmem_limit_bytes=VMEM_GRANT
         ),

time: 51.2 us -> 50.9 us (level)
  no operation moved by 1% of the time
where the time goes in v4:
time: 50.9 us; the launch traced here: 50.8 us
  Pallas kernels  50 us (98%)
  between operations  0.74 us (1%)
    pallas_call x1, Pallas kernels, per_device(): pl.pallas_call(functools.partial(fused_kernel, nf, nr, nt), out_shape=tup...  47.4 us
    pallas_call x1, Pallas kernels, per_device(): pl.pallas_call(closing_kernel, grid=(nr,), out_shape=tuple((jax.ShapeDtyp...  2.64 us

profile of v4, /device:TPU:0, one launch (start us, length us, event | category | flops | bytes accessed | tf_op | source)
XLA Modules:
  0.0 50.8 jit_solution(1990584013397841372)
XLA Ops:
  0.6 0.0 copy-start.3
  0.6 0.0 copy-start.2
  0.7 0.0 copy-start.1
  0.7 0.0 copy-start.5
  0.7 0.0 copy-start.4
  0.7 0.0 copy-start
  0.7 47.4 %shard_map.161 = (bf16[4,128,512]{2,1,0:T(8,128)(2,1)S(1)}, bf16[4,64,512]{2,1,0:T(8,128)(2,1)S(1)}, f32[8,128]{1,0:T(8,128)S(1)}, f32[64,512]{1,0:T(8,128)S(1)}, f32[4,4,8,128]{3,2,1,0:T(8,128)S(1)}) custom-call(bf16[768,2048]{1,0:T(8,128)(2,1)} %x_hbm.1, bf16[768,512]{1,0:T(8,128)(2,1)} %c_hbm.1, f32[8,768]{1,0:T(8,128)} %gc_hbm.1, f32[8,768]{1,0:T(8,128)} %gt_hbm.1, ...), custom_call_target="tpu_custom_call" | custom-call | tf_op jit(solution)/shard_map/pallas_call | solution.py:497
  48.1 0.0 copy-done.3
  48.1 0.0 copy-done.2
  48.1 0.0 copy-done.1
  48.1 0.0 copy-done.5
  48.1 0.0 copy-done.4
  48.1 0.0 copy-done
  48.1 2.6 %shard_map.162 = (f32[512,512]{1,0:T(8,128)}, f32[512,512]{1,0:T(8,128)}, bf16[512,512]{1,0:T(8,128)(2,1)}, f32[64,512]{1,0:T(8,128)}, f32[64,512]{1,0:T(8,128)}...) custom-call(bf16[4,128,512]{2,1,0:T(8,128)(2,1)S(1)} %get-tuple-element.13.g_ref, ...), custom_call_target="tpu_custom_call" | custom-call | tf_op jit(solution)/shard_map/pallas_call | solution.py:515
Async XLA Ops:
  0.6 47.5 %copy-start.3 = (f32[64,512]{1,0:T(8,128)S(1)}, f32[64,512]{1,0:T(8,128)}, u32[]{:S(2)}) copy-start(f32[64,512]{1,0:T(8,128)} %ls_ref.1) | copy-start | bytes 393220
  0.6 47.5 %copy-start.2 = (f32[64,512]{1,0:T(8,128)S(1)}, f32[64,512]{1,0:T(8,128)}, u32[]{:S(2)}) copy-start(f32[64,512]{1,0:T(8,128)} %lm_ref.1) | copy-start | bytes 393220
  0.7 47.5 %copy-start.1 = (bf16[512,256]{1,0:T(8,128)(2,1)S(1)}, bf16[512,256]{1,0:T(8,128)(2,1)}, u32[]{:S(2)}) copy-start(bf16[512,256]{1,0:T(8,128)(2,1)} %pj_ref.1) | copy-start | bytes 786436
  0.7 47.5 %copy-start.5 = (f32[8,2048]{1,0:T(8,128)S(1)}, f32[8,2048]{1,0:T(8,128)}, u32[]{:S(2)}) copy-start(f32[8,2048]{1,0:T(8,128)} %gq_ref.1) | copy-start | bytes 196612
  0.7 47.5 %copy-start.4 = (f32[8,2048]{1,0:T(8,128)S(1)}, f32[8,2048]{1,0:T(8,128)}, u32[]{:S(2)}) copy-start(f32[8,2048]{1,0:T(8,128)} %gm_ref.1) | copy-start | bytes 196612
  0.7 47.5 %copy-start = (f32[512,512]{1,0:T(8,128)S(1)}, f32[512,512]{1,0:T(8,128)}, u32[]{:S(2)}) copy-start(f32[512,512]{1,0:T(8,128)} %qm_ref.1) | copy-start | bytes 3145732

commit v5 on v4

--- a/solution.py
+++ b/solution.py
@@ -102,7 +102,7 @@
     x_ref, c_ref, c_twin, gc_ref, gt_ref, lm_ref, ls_ref, p_all,
     a_send, a_recv, a_own, a_keep, m_send, m_recv, b_send, b_recv, g_ref,
     xp_ref, d_send, d_recv, e_all, f_send, f_recv,
-    ra_send, ra_recv, rb_part, rb_recv, rc_all,
+    ra_send, ra_recv, rb_all,
     send_sem, recv_sem, load_sem,
 ):
     f, r, t = lax.axis_index("fs"), lax.axis_index("rep"), lax.axis_index("tp")
@@ -155,11 +155,17 @@
     def rep(k):
         return (f, square[k], t)
 
-    def depth(k):
-        return (lax.rem(f + k, nf), r, t)
+    def place(n):
+        up = jnp.where(f <= n, n + 1, n)
+        down = jnp.where(f <= nf - 2 - n, nf - 1 - n, nf - 2 - n)
+        return jnp.where(2 * f < nf, up, down)
+
+    def spread(group, key, src, dst):
+        for n in reversed(range(nf - 1)):
+            send(group, key, src, dst, (place(n), r, t))
 
     spots = [(f, square[k], lax.rem(t + dt, nt)) for k in range(4) for dt in range(nt) if k or dt]
-    peers = [depth(k) for k in fss] + spots
+    peers = [(place(n), r, t) for n in range(nf - 1)] + spots
     barrier = pltpu.get_barrier_semaphore()
     for peer in peers:
         pl.semaphore_signal(barrier, inc=1, device_id=peer, device_id_type=MESH)
@@ -219,19 +225,19 @@
                 + m_recv[p, h, j].astype(fl)
             )
 
-        for k in fss:
+        for n in reversed(range(nf - 1)):
             for h in range(2):
-                b_send[p, k - 1, h] = summed(h, lax.rem(f + k, nf)).astype(bf)
-            send("third", ("third", p), b_send.at[p, k - 1], b_recv.at[p, k - 1], depth(k))
+                b_send[p, n, h] = summed(h, place(n)).astype(bf)
+            send("third", ("third", p), b_send.at[p, n], b_recv.at[p, f], (place(n), r, t))
         for h in range(2):
             g_ref[h, :, cut(p)] = summed(h, f)
 
     def send_fourth(p):
-        arrive(("third", p), b_recv.at[p])
+        arrive(("third", p), b_recv.at[p, : nf - 1])
         for h in range(2):
             total = g_ref[h, :, cut(p)]
-            for k in fss:
-                total = total + b_recv[p, k - 1, h].astype(fl)
+            for n in range(nf - 1):
+                total = total + b_recv[p, place(n), h].astype(fl)
             g_all[r, h * half : (h + 1) * half, cut(p)] = (total * norming).astype(bf)
         where = g_all.at[r, :, cut(p)]
         for k in squares:
@@ -242,8 +248,14 @@
     fill(3, 1)
     settle(load_sem.at[nr + 1], p_all.at[0])
     pl.semaphore_wait(barrier, len(peers))
-    for k in fss:
-        send("cast", ("cast", k), p_all.at[f], p_all.at[f], depth(k))
+    cast_sem = 3 * PIECES + 10
+    for n in reversed(range(nf - 1)):
+        pltpu.make_async_remote_copy(
+            src_ref=p_all.at[f], dst_ref=p_all.at[f],
+            send_sem=send_sem.at[groups.setdefault("cast", len(groups))],
+            recv_sem=recv_sem.at[cast_sem + f],
+            device_id=(place(n), r, t), device_id_type=MESH,
+        ).start()
     send("twin", "twin", c_ref, c_twin, (f, r, 1 - t))
     for j in range(2, nf):
         fill(3, j)
@@ -262,11 +274,10 @@
     send_first(2)
 
     def cast(q):
-        place = lax.rem(f + q, nf)
-        where = pl.ds(pl.multiple_of(place * nr * thin, nr * thin), nr * thin)
-        return jnp.dot(x_ref[:, where], p_all[place], preferred_element_type=fl)
-
-    xp_ref[...] = cast(0)
+        where = pl.ds(pl.multiple_of(q * nr * thin, nr * thin), nr * thin)
+        return jnp.dot(x_ref[:, where], p_all[q], preferred_element_type=fl)
+
+    xp_ref[...] = cast(f)
 
     for i, ref in enumerate((gc_ref, gt_ref, lm_ref, ls_ref)):
         settle(load_sem.at[nr + 2 + i], ref)
@@ -303,12 +314,17 @@
     for k in squares:
         send("ra", "ra", ra_send.at[square[k]], ra_recv.at[k - 1], rep(k))
 
-    for k in fss[:-1]:
-        arrive(("cast", k), p_all.at[0])
-        xp_ref[...] += cast(nf - k)
+    def arrive_cast(n):
+        settle(recv_sem.at[cast_sem + place(n)], p_all.at[0])
+        return cast(place(n))
+
+    xp_ref[...] += arrive_cast(0)
     send_second(1)
-    arrive(("cast", nf - 1), p_all.at[0])
-    cast_all = xp_ref[...] + cast(1)
+    send_first(3)
+    for n in range(1, nf - 2):
+        xp_ref[...] += arrive_cast(n)
+    send_third(0)
+    cast_all = xp_ref[...] + arrive_cast(nf - 2)
     high = cast_all.astype(bf)
     low = (cast_all - high.astype(fl)).astype(bf)
     arrive("twin", c_twin)
@@ -336,8 +352,12 @@
                 send("d1", "d", d_send.at[0, 0], d_recv.at[2], rep(2))
 
     send_second(2)
-    send_first(3)
-    send_third(0)
+    arrive("ra", ra_recv)
+    gate_rows = ra_send[r]
+    for k in squares:
+        gate_rows = gate_rows + ra_recv[k - 1]
+    rb_all[f] = gate_rows
+    spread("rb", "rb", rb_all.at[f], rb_all.at[f])
     send_third(1)
 
     @pl.when(crossed == 0)
@@ -352,28 +372,12 @@
     for k in squares:
         total = total + d_recv[k].astype(fl)
     e_all[f] = total.astype(bf)
-    for k in fss:
-        send("e", "e", e_all.at[f], e_all.at[f], depth(k))
-
-    arrive("ra", ra_recv)
-    gate_rows = ra_send[r]
-    for k in squares:
-        gate_rows = gate_rows + ra_recv[k - 1]
-    rb_part[...] = gate_rows
-    for k in fss:
-        send("rb", "rb", rb_part.at[lax.rem(f + k, nf)], rb_recv.at[k - 1], depth(k))
-
+    spread("e", "e", e_all.at[f], e_all.at[f])
     send_fourth(0)
+    send_second(3)
     send_third(2)
-    send_second(3)
     send_fourth(1)
-    arrive("rb", rb_recv)
-    gate_block = rb_part[f]
-    for k in fss:
-        gate_block = gate_block + rb_recv[k - 1]
-    rc_all[f] = gate_block * norming
-    for k in fss:
-        send("rc", "rc", rc_all.at[f], rc_all.at[f], depth(k))
+    send_third(3)
 
     arrive("e", e_all.at[: nf - 1])
     projected = e_all[0].astype(fl)
@@ -387,7 +391,6 @@
     for i, spot in enumerate(spots):
         send("f", "f", f_send, f_recv.at[i], spot)
     projected_ref[...] = projected
-    send_third(3)
     arrive("f", f_recv)
     sums = f_send[...]
     for i in range(len(spots)):
@@ -399,8 +402,11 @@
         send("h", "h", h_all.at[r], h_all.at[r], rep(k))
 
     send_fourth(2)
-    arrive("rc", rc_all.at[: nf - 1])
-    rd_all[r] = rc_all[...]
+    arrive("rb", rb_all.at[: nf - 1])
+    gate_block = rb_all[0]
+    for j in fss:
+        gate_block = gate_block + rb_all[j]
+    rd_all[r] = gate_block * norming
     for k in squares:
         send("rd", "rd", rd_all.at[r], rd_all.at[r], rep(k))
     send_fourth(3)
@@ -411,7 +417,7 @@
         "first": a_send, "cast": p_all.at[: nf - 1], "twin": c_ref, "second": m_send,
         "third": b_send, "fourth": g_all.at[: nr - 1], "d": d_recv.at[: nr - 1],
         "e": e_all.at[: nf - 1], "f": f_recv, "h": h_all.at[: nr - 1], "ra": ra_recv,
-        "rb": rb_recv, "rc": rc_all.at[: nf - 1], "rd": rd_all.at[: nr - 1],
+        "rb": rb_all.at[: nf - 1], "rd": rd_all.at[: nr - 1],
     }
     for group, ref in sent.items():
         settle(send_sem.at[groups[group]], ref)
@@ -462,7 +468,7 @@
     thin = width // (nf * nr)
     fits = (
         width % (nf * nr * 128) == 0 and rank_rows % 16 == 0
-        and cols % (PIECES * 128) == 0 and heads % 8 == 0 and nf > 1 and nr == 4 and nt == 2
+        and cols % (PIECES * 128) == 0 and heads % 8 == 0 and nf > 2 and nr == 4 and nt == 2
         and x.shape[0] % 128 == 0 and rank_all % (nt * 128) == 0
     )
     if not fits:
@@ -474,14 +480,13 @@
         ((PIECES, 2, 2, nf, half, piece), bf), ((PIECES, 2, 2, nf, half, piece), bf),
         ((nf, thin, cols), fl), ((2, nf, half, cols), fl),
         ((PIECES, 2, nf, half, piece), bf), ((PIECES, 2, nf, half, piece), bf),
-        ((PIECES, nf - 1, 2, half, piece), bf), ((PIECES, nf - 1, 2, half, piece), bf),
+        ((PIECES, nf - 1, 2, half, piece), bf), ((PIECES, nf, 2, half, piece), bf),
         ((2, half, cols), fl),
         ((x.shape[0], rank_all // nt), fl),
         ((2, nt, rank_rows, cols), bf), ((nr, rank_rows, cols), bf),
         ((nf, rank_rows, cols), bf), ((8, 128), fl), ((nr * nt - 1, 8, 128), fl),
         ((nr, nf, heads, thin), fl), ((nr - 1, nf, heads, thin), fl),
-        ((nf, heads, thin), fl), ((nf - 1, heads, thin), fl),
-        ((nf, heads, thin), fl),
+        ((nf, nf, heads, thin), fl),
     ]
     outs = [
         (qm.shape, fl), (qm.shape, fl), (qm.shape, bf), (lm.shape, fl), (lm.shape, fl),
@@ -493,7 +498,7 @@
     ]
     vmem = pl.BlockSpec(memory_space=pltpu.VMEM)
     hbm = pl.BlockSpec(memory_space=pltpu.HBM)
-    semaphores = (15, 3 * PIECES + nf + 10, nr + 6)
+    semaphores = (14, 3 * PIECES + 10 + nf, nr + 6)
     passed = pl.pallas_call(
         functools.partial(fused_kernel, nf, nr, nt),
         out_shape=tuple(jax.ShapeDtypeStruct(*o) for o in between),

time: 50.9 us -> 50.8 us (level)
  the two profiles are of different devices: /device:TPU:0 before, /device:TPU:8 now
where the time goes in v5:
time: 50.8 us; the launch traced here: 50.7 us
  Pallas kernels  49.9 us (98%)
  between operations  0.74 us (1%)
    pallas_call x1, Pallas kernels, per_device(): pl.pallas_call(functools.partial(fused_kernel, nf, nr, nt), out_shape=tup...  47.3 us
    pallas_call x1, Pallas kernels, per_device(): pl.pallas_call(closing_kernel, grid=(nr,), out_shape=tuple((jax.ShapeDtyp...  2.64 us

profile of v5, /device:TPU:8, one launch (start us, length us, event | category | flops | bytes accessed | tf_op | source)
XLA Modules:
  0.0 50.7 jit_solution(10677239573779220590)
XLA Ops:
  0.6 0.0 copy-start.3
  0.6 0.0 copy-start.2
  0.7 0.0 copy-start.1
  0.7 0.0 copy-start.5
  0.7 0.0 copy-start.4
  0.7 0.0 copy-start
  0.7 47.3 %shard_map.161 = (bf16[4,128,512]{2,1,0:T(8,128)(2,1)S(1)}, bf16[4,64,512]{2,1,0:T(8,128)(2,1)S(1)}, f32[8,128]{1,0:T(8,128)S(1)}, f32[64,512]{1,0:T(8,128)S(1)}, f32[4,4,8,128]{3,2,1,0:T(8,128)S(1)}) custom-call(bf16[768,2048]{1,0:T(8,128)(2,1)} %x_hbm.1, bf16[768,512]{1,0:T(8,128)(2,1)} %c_hbm.1, f32[8,768]{1,0:T(8,128)} %gc_hbm.1, f32[8,768]{1,0:T(8,128)} %gt_hbm.1, ...), custom_call_target="tpu_custom_call" | custom-call | tf_op jit(solution)/shard_map/pallas_call | solution.py:502
  48.0 0.0 copy-done.3
  48.0 0.0 copy-done.2
  48.0 0.0 copy-done.1
  48.0 0.0 copy-done.5
  48.0 0.0 copy-done.4
  48.0 0.0 copy-done
  48.0 2.6 %shard_map.162 = (f32[512,512]{1,0:T(8,128)}, f32[512,512]{1,0:T(8,128)}, bf16[512,512]{1,0:T(8,128)(2,1)}, f32[64,512]{1,0:T(8,128)}, f32[64,512]{1,0:T(8,128)}...) custom-call(bf16[4,128,512]{2,1,0:T(8,128)(2,1)S(1)} %get-tuple-element.13.g_ref, ...), custom_call_target="tpu_custom_call" | custom-call | tf_op jit(solution)/shard_map/pallas_call | solution.py:520
Async XLA Ops:
  0.6 47.3 %copy-start.3 = (f32[64,512]{1,0:T(8,128)S(1)}, f32[64,512]{1,0:T(8,128)}, u32[]{:S(2)}) copy-start(f32[64,512]{1,0:T(8,128)} %ls_ref.1) | copy-start | bytes 393220
  0.6 47.3 %copy-start.2 = (f32[64,512]{1,0:T(8,128)S(1)}, f32[64,512]{1,0:T(8,128)}, u32[]{:S(2)}) copy-start(f32[64,512]{1,0:T(8,128)} %lm_ref.1) | copy-start | bytes 393220
  0.7 47.3 %copy-start.1 = (bf16[512,256]{1,0:T(8,128)(2,1)S(1)}, bf16[512,256]{1,0:T(8,128)(2,1)}, u32[]{:S(2)}) copy-start(bf16[512,256]{1,0:T(8,128)(2,1)} %pj_ref.1) | copy-start | bytes 786436
  0.7 47.3 %copy-start.5 = (f32[8,2048]{1,0:T(8,128)S(1)}, f32[8,2048]{1,0:T(8,128)}, u32[]{:S(2)}) copy-start(f32[8,2048]{1,0:T(8,128)} %gq_ref.1) | copy-start | bytes 196612
  0.7 47.3 %copy-start.4 = (f32[8,2048]{1,0:T(8,128)S(1)}, f32[8,2048]{1,0:T(8,128)}, u32[]{:S(2)}) copy-start(f32[8,2048]{1,0:T(8,128)} %gm_ref.1) | copy-start | bytes 196612
  0.7 47.3 %copy-start = (f32[512,512]{1,0:T(8,128)S(1)}, f32[512,512]{1,0:T(8,128)}, u32[]{:S(2)}) copy-start(f32[512,512]{1,0:T(8,128)} %qm_ref.1) | copy-start | bytes 3145732

commit v6 on v5

--- a/solution.py
+++ b/solution.py
@@ -100,7 +100,7 @@
     x_hbm, c_hbm, gc_hbm, gt_hbm, pj_hbm, lm_hbm, ls_hbm,
     g_all, h_all, balance_ref, projected_ref, rd_all,
     x_ref, c_ref, c_twin, gc_ref, gt_ref, lm_ref, ls_ref, p_all,
-    a_send, a_recv, a_own, a_keep, m_send, m_recv, b_send, b_recv, g_ref,
+    a_send, a_recv, a_own, a_keep, m_send, m_recv, b_send, b_recv, v_send, v_recv,
     xp_ref, d_send, d_recv, e_all, f_send, f_recv,
     ra_send, ra_recv, rb_all,
     send_sem, recv_sem, load_sem,
@@ -213,31 +213,35 @@
                 m_send[p, h, j] = value.astype(bf)
             send("second", ("second", p), m_send.at[p, h], m_recv.at[p, h], rep(2 - h))
 
+    mate = f + 1 - 2 * lax.rem(f, 2)
+    over = lax.rem(f + nf // 2, nf)
+    mate_over = lax.rem(mate + nf // 2, nf)
+
+    def summed(p, h, j):
+        rows = slice(h * half, (h + 1) * half)
+        return (
+            a_own[j, rows, cut(p)] + a_recv[p, h, 1, j].astype(fl) + m_recv[p, h, j].astype(fl)
+        )
+
     def send_third(p):
         if p == 0:
             arrive(("open", 1), a_recv.at[0, :, 1])
         arrive(("second", p), m_recv.at[p])
-
-        def summed(h, j):
-            rows = slice(h * half, (h + 1) * half)
-            return (
-                a_own[j, rows, cut(p)] + a_recv[p, h, 1, j].astype(fl)
-                + m_recv[p, h, j].astype(fl)
-            )
-
-        for n in reversed(range(nf - 1)):
+        for o, j in enumerate((mate_over, mate)):
             for h in range(2):
-                b_send[p, n, h] = summed(h, place(n)).astype(bf)
-            send("third", ("third", p), b_send.at[p, n], b_recv.at[p, f], (place(n), r, t))
+                b_send[p, o, h] = summed(p, h, j).astype(bf)
+        send("third", ("third", p), b_send.at[p], b_recv.at[p], (mate, r, t))
+
+    def send_cross(p):
+        arrive(("third", p), b_recv.at[p])
         for h in range(2):
-            g_ref[h, :, cut(p)] = summed(h, f)
+            v_send[p, h] = (summed(p, h, over) + b_recv[p, 0, h].astype(fl)).astype(bf)
+        send("cross", ("cross", p), v_send.at[p], v_recv.at[p], (over, r, t))
 
     def send_fourth(p):
-        arrive(("third", p), b_recv.at[p, : nf - 1])
+        arrive(("cross", p), v_recv.at[p])
         for h in range(2):
-            total = g_ref[h, :, cut(p)]
-            for n in range(nf - 1):
-                total = total + b_recv[p, place(n), h].astype(fl)
+            total = summed(p, h, f) + b_recv[p, 1, h].astype(fl) + v_recv[p, h].astype(fl)
             g_all[r, h * half : (h + 1) * half, cut(p)] = (total * norming).astype(bf)
         where = g_all.at[r, :, cut(p)]
         for k in squares:
@@ -248,14 +252,47 @@
     fill(3, 1)
     settle(load_sem.at[nr + 1], p_all.at[0])
     pl.semaphore_wait(barrier, len(peers))
-    cast_sem = 3 * PIECES + 10
-    for n in reversed(range(nf - 1)):
+    inner = f * (nf - 1 - f) > 0
+    cast_sem = 4 * PIECES + 10
+    deep = p_all.shape[1] // 2
+
+    def leaf(q, i):
+        return p_all.at[q, i * deep : (i + 1) * deep]
+
+    def cast_arrive(q, i):
+        settle(recv_sem.at[cast_sem + 2 * q + i], leaf(0, i))
+
+    def cast_send(group, q, i, where):
         pltpu.make_async_remote_copy(
-            src_ref=p_all.at[f], dst_ref=p_all.at[f],
-            send_sem=send_sem.at[groups.setdefault("cast", len(groups))],
-            recv_sem=recv_sem.at[cast_sem + f],
-            device_id=(place(n), r, t), device_id_type=MESH,
+            src_ref=leaf(q, i), dst_ref=leaf(q, i),
+            send_sem=send_sem.at[groups.setdefault(group, len(groups))],
+            recv_sem=recv_sem.at[cast_sem + 2 * q + i],
+            device_id=(where, r, t), device_id_type=MESH,
         ).start()
+
+    def relay(hop, i):
+        @pl.when(inner)
+        def _():
+            if hop == 1:
+                cast_arrive(f - 1, i)
+                cast_send("cast", f - 1, i, f + 1)
+                cast_arrive(f + 1, i)
+                cast_send("cast", f + 1, i, f - 1)
+            else:
+                cast_arrive(over, i)
+                cast_send("cast2", over, i, (nf - 1) * (f - 1))
+
+    @pl.when(inner)
+    def _():
+        for i in range(2):
+            cast_send("cast", f, i, f - 1)
+            cast_send("cast", f, i, f + 1)
+
+    @pl.when(jnp.logical_not(inner))
+    def _():
+        for i in range(2):
+            cast_send("cast", f, i, place(0))
+
     send("twin", "twin", c_ref, c_twin, (f, r, 1 - t))
     for j in range(2, nf):
         fill(3, j)
@@ -270,6 +307,7 @@
     ready(0)
     for j in range(nf):
         fill(0, j)
+    relay(1, 0)
     send_second(0)
     send_first(2)
 
@@ -278,6 +316,7 @@
         return jnp.dot(x_ref[:, where], p_all[q], preferred_element_type=fl)
 
     xp_ref[...] = cast(f)
+    relay(1, 1)
 
     for i, ref in enumerate((gc_ref, gt_ref, lm_ref, ls_ref)):
         settle(load_sem.at[nr + 2 + i], ref)
@@ -314,17 +353,21 @@
     for k in squares:
         send("ra", "ra", ra_send.at[square[k]], ra_recv.at[k - 1], rep(k))
 
+    relay(2, 0)
+    send_second(1)
+    relay(2, 1)
+    send_third(0)
+
     def arrive_cast(n):
-        settle(recv_sem.at[cast_sem + place(n)], p_all.at[0])
+        @pl.when(jnp.logical_not(inner))
+        def _():
+            for i in range(2):
+                cast_arrive(place(n), i)
         return cast(place(n))
 
     xp_ref[...] += arrive_cast(0)
-    send_second(1)
-    send_first(3)
-    for n in range(1, nf - 2):
-        xp_ref[...] += arrive_cast(n)
-    send_third(0)
-    cast_all = xp_ref[...] + arrive_cast(nf - 2)
+    xp_ref[...] += arrive_cast(1)
+    cast_all = xp_ref[...] + arrive_cast(2)
     high = cast_all.astype(bf)
     low = (cast_all - high.astype(fl)).astype(bf)
     arrive("twin", c_twin)
@@ -352,13 +395,15 @@
                 send("d1", "d", d_send.at[0, 0], d_recv.at[2], rep(2))
 
     send_second(2)
+    send_first(3)
+    send_cross(0)
+    send_third(1)
     arrive("ra", ra_recv)
     gate_rows = ra_send[r]
     for k in squares:
         gate_rows = gate_rows + ra_recv[k - 1]
     rb_all[f] = gate_rows
     spread("rb", "rb", rb_all.at[f], rb_all.at[f])
-    send_third(1)
 
     @pl.when(crossed == 0)
     def _():
@@ -373,11 +418,11 @@
         total = total + d_recv[k].astype(fl)
     e_all[f] = total.astype(bf)
     spread("e", "e", e_all.at[f], e_all.at[f])
+    send_cross(1)
     send_fourth(0)
+    send_third(2)
     send_second(3)
-    send_third(2)
-    send_fourth(1)
-    send_third(3)
+    send_cross(2)
 
     arrive("e", e_all.at[: nf - 1])
     projected = e_all[0].astype(fl)
@@ -391,6 +436,8 @@
     for i, spot in enumerate(spots):
         send("f", "f", f_send, f_recv.at[i], spot)
     projected_ref[...] = projected
+    send_fourth(1)
+    send_third(3)
     arrive("f", f_recv)
     sums = f_send[...]
     for i in range(len(spots)):
@@ -409,18 +456,28 @@
     rd_all[r] = gate_block * norming
     for k in squares:
         send("rd", "rd", rd_all.at[r], rd_all.at[r], rep(k))
+    send_cross(3)
     send_fourth(3)
     arrive("rd", rd_all.at[: nr - 1])
     arrive("h", h_all.at[: nr - 1])
     arrive("fourth", g_all.at[: nr - 1])
     sent = {
-        "first": a_send, "cast": p_all.at[: nf - 1], "twin": c_ref, "second": m_send,
-        "third": b_send, "fourth": g_all.at[: nr - 1], "d": d_recv.at[: nr - 1],
+        "first": a_send, "twin": c_ref, "second": m_send,
+        "third": b_send, "cross": v_send, "fourth": g_all.at[: nr - 1], "d": d_recv.at[: nr - 1],
         "e": e_all.at[: nf - 1], "f": f_recv, "h": h_all.at[: nr - 1], "ra": ra_recv,
         "rb": rb_all.at[: nf - 1], "rd": rd_all.at[: nr - 1],
     }
     for group, ref in sent.items():
         settle(send_sem.at[groups[group]], ref)
+
+    @pl.when(inner)
+    def _():
+        settle(send_sem.at[groups["cast"]], p_all)
+        settle(send_sem.at[groups["cast2"]], p_all.at[0])
+
+    @pl.when(jnp.logical_not(inner))
+    def _():
+        settle(send_sem.at[groups["cast"]], p_all.at[0])
 
     @pl.when(crossed == 1)
     def _():
@@ -468,7 +525,7 @@
     thin = width // (nf * nr)
     fits = (
         width % (nf * nr * 128) == 0 and rank_rows % 16 == 0
-        and cols % (PIECES * 128) == 0 and heads % 8 == 0 and nf > 2 and nr == 4 and nt == 2
+        and cols % (PIECES * 128) == 0 and heads % 8 == 0 and nf == 4 and nr == 4 and nt == 2
         and x.shape[0] % 128 == 0 and rank_all % (nt * 128) == 0
     )
     if not fits:
@@ -480,8 +537,8 @@
         ((PIECES, 2, 2, nf, half, piece), bf), ((PIECES, 2, 2, nf, half, piece), bf),
         ((nf, thin, cols), fl), ((2, nf, half, cols), fl),
         ((PIECES, 2, nf, half, piece), bf), ((PIECES, 2, nf, half, piece), bf),
-        ((PIECES, nf - 1, 2, half, piece), bf), ((PIECES, nf, 2, half, piece), bf),
-        ((2, half, cols), fl),
+        ((PIECES, 2, 2, half, piece), bf), ((PIECES, 2, 2, half, piece), bf),
+        ((PIECES, 2, half, piece), bf), ((PIECES, 2, half, piece), bf),
         ((x.shape[0], rank_all // nt), fl),
         ((2, nt, rank_rows, cols), bf), ((nr, rank_rows, cols), bf),
         ((nf, rank_rows, cols), bf), ((8, 128), fl), ((nr * nt - 1, 8, 128), fl),
@@ -498,7 +555,7 @@
     ]
     vmem = pl.BlockSpec(memory_space=pltpu.VMEM)
     hbm = pl.BlockSpec(memory_space=pltpu.HBM)
-    semaphores = (14, 3 * PIECES + 10 + nf, nr + 6)
+    semaphores = (16, 4 * PIECES + 10 + 2 * nf, nr + 6)
     passed = pl.pallas_call(
         functools.partial(fused_kernel, nf, nr, nt),
         out_shape=tuple(jax.ShapeDtypeStruct(*o) for o in between),

time: 50.8 us -> 47.6 us (0.937)
  the two profiles are of different devices: /device:TPU:8 before, /device:TPU:0 now
where the time goes in v6:
time: 47.6 us; the launch traced here: 47.5 us
  Pallas kernels  46.7 us (98%)
  between operations  0.74 us (2%)
    pallas_call x1, Pallas kernels, per_device(): pl.pallas_call(functools.partial(fused_kernel, nf, nr, nt), out_shape=tup...  44.1 us
    pallas_call x1, Pallas kernels, per_device(): pl.pallas_call(closing_kernel, grid=(nr,), out_shape=tuple((jax.ShapeDtyp...  2.64 us

profile of v6, /device:TPU:0, one launch (start us, length us, event | category | flops | bytes accessed | tf_op | source)
XLA Modules:
  0.0 47.5 jit_solution(278869794972619027)
XLA Ops:
  0.6 0.0 copy-start.3
  0.6 0.0 copy-start.2
  0.7 0.0 copy-start.1
  0.7 0.0 copy-start.5
  0.7 0.0 copy-start.4
  0.7 0.0 copy-start
  0.7 44.1 %shard_map.161 = (bf16[4,128,512]{2,1,0:T(8,128)(2,1)S(1)}, bf16[4,64,512]{2,1,0:T(8,128)(2,1)S(1)}, f32[8,128]{1,0:T(8,128)S(1)}, f32[64,512]{1,0:T(8,128)S(1)}, f32[4,4,8,128]{3,2,1,0:T(8,128)S(1)}) custom-call(bf16[768,2048]{1,0:T(8,128)(2,1)} %x_hbm.1, bf16[768,512]{1,0:T(8,128)(2,1)} %c_hbm.1, f32[8,768]{1,0:T(8,128)} %gc_hbm.1, f32[8,768]{1,0:T(8,128)} %gt_hbm.1, ...), custom_call_target="tpu_custom_call" | custom-call | tf_op jit(solution)/shard_map/pallas_call | solution.py:559
  44.8 0.0 copy-done.3
  44.8 0.0 copy-done.2
  44.8 0.0 copy-done.1
  44.8 0.0 copy-done.5
  44.8 0.0 copy-done.4
  44.8 0.0 copy-done
  44.8 2.6 %shard_map.162 = (f32[512,512]{1,0:T(8,128)}, f32[512,512]{1,0:T(8,128)}, bf16[512,512]{1,0:T(8,128)(2,1)}, f32[64,512]{1,0:T(8,128)}, f32[64,512]{1,0:T(8,128)}...) custom-call(bf16[4,128,512]{2,1,0:T(8,128)(2,1)S(1)} %get-tuple-element.13.g_ref, ...), custom_call_target="tpu_custom_call" | custom-call | tf_op jit(solution)/shard_map/pallas_call | solution.py:577
Async XLA Ops:
  0.6 44.1 %copy-start.3 = (f32[64,512]{1,0:T(8,128)S(1)}, f32[64,512]{1,0:T(8,128)}, u32[]{:S(2)}) copy-start(f32[64,512]{1,0:T(8,128)} %ls_ref.1) | copy-start | bytes 393220
  0.6 44.1 %copy-start.2 = (f32[64,512]{1,0:T(8,128)S(1)}, f32[64,512]{1,0:T(8,128)}, u32[]{:S(2)}) copy-start(f32[64,512]{1,0:T(8,128)} %lm_ref.1) | copy-start | bytes 393220
  0.7 44.1 %copy-start.1 = (bf16[512,256]{1,0:T(8,128)(2,1)S(1)}, bf16[512,256]{1,0:T(8,128)(2,1)}, u32[]{:S(2)}) copy-start(bf16[512,256]{1,0:T(8,128)(2,1)} %pj_ref.1) | copy-start | bytes 786436
  0.7 44.1 %copy-start.5 = (f32[8,2048]{1,0:T(8,128)S(1)}, f32[8,2048]{1,0:T(8,128)}, u32[]{:S(2)}) copy-start(f32[8,2048]{1,0:T(8,128)} %gq_ref.1) | copy-start | bytes 196612
  0.7 44.1 %copy-start.4 = (f32[8,2048]{1,0:T(8,128)S(1)}, f32[8,2048]{1,0:T(8,128)}, u32[]{:S(2)}) copy-start(f32[8,2048]{1,0:T(8,128)} %gm_ref.1) | copy-start | bytes 196612
  0.7 44.1 %copy-start = (f32[512,512]{1,0:T(8,128)S(1)}, f32[512,512]{1,0:T(8,128)}, u32[]{:S(2)}) copy-start(f32[512,512]{1,0:T(8,128)} %qm_ref.1) | copy-start | bytes 3145732

commit v7 on v6

--- a/solution.py
+++ b/solution.py
@@ -15,6 +15,7 @@
 
 
 PIECES = 4
+LEAVES = 4
 VMEM_GRANT = 32 * 1024 * 1024
 MESH = pl.DeviceIdType.MESH
 CONTRACT = (((0,), (0,)), ((), ()))
@@ -129,8 +130,8 @@
         pltpu.make_async_copy(ref, ref, sem).wait()
 
     mine = pl.ds(pl.multiple_of(t * rank_half, rank_half), rank_half)
+    load(nr + 1, pj_hbm.at[:, mine], p_all.at[f])
     load(nr, c_hbm, c_ref)
-    load(nr + 1, pj_hbm.at[:, mine], p_all.at[f])
     for k in [3, 1, 2, 0]:
         for j in range(nf):
             where = columns(square[k], j)
@@ -169,8 +170,6 @@
     barrier = pltpu.get_barrier_semaphore()
     for peer in peers:
         pl.semaphore_signal(barrier, inc=1, device_id=peer, device_id_type=MESH)
-
-    settle(load_sem.at[nr], c_ref)
 
     def cut(p):
         return slice(p * piece, (p + 1) * piece)
@@ -247,54 +246,57 @@
         for k in squares:
             send("fourth", "fourth", where, where, rep(k))
 
-    ready(3)
-    fill(3, 0)
-    fill(3, 1)
     settle(load_sem.at[nr + 1], p_all.at[0])
     pl.semaphore_wait(barrier, len(peers))
     inner = f * (nf - 1 - f) > 0
     cast_sem = 4 * PIECES + 10
-    deep = p_all.shape[1] // 2
+    deep = p_all.shape[1] // LEAVES
 
     def leaf(q, i):
         return p_all.at[q, i * deep : (i + 1) * deep]
 
     def cast_arrive(q, i):
-        settle(recv_sem.at[cast_sem + 2 * q + i], leaf(0, i))
+        settle(recv_sem.at[cast_sem + LEAVES * q + i], leaf(0, i))
 
     def cast_send(group, q, i, where):
         pltpu.make_async_remote_copy(
             src_ref=leaf(q, i), dst_ref=leaf(q, i),
             send_sem=send_sem.at[groups.setdefault(group, len(groups))],
-            recv_sem=recv_sem.at[cast_sem + 2 * q + i],
+            recv_sem=recv_sem.at[cast_sem + LEAVES * q + i],
             device_id=(where, r, t), device_id_type=MESH,
         ).start()
 
-    def relay(hop, i):
+    def relay(hop, leaves):
         @pl.when(inner)
         def _():
-            if hop == 1:
-                cast_arrive(f - 1, i)
-                cast_send("cast", f - 1, i, f + 1)
-                cast_arrive(f + 1, i)
-                cast_send("cast", f + 1, i, f - 1)
-            else:
-                cast_arrive(over, i)
-                cast_send("cast2", over, i, (nf - 1) * (f - 1))
+            for i in leaves:
+                relay_leaf(hop, i)
+
+    def relay_leaf(hop, i):
+        if hop == 1:
+            cast_arrive(f - 1, i)
+            cast_send("cast", f - 1, i, f + 1)
+            cast_arrive(f + 1, i)
+            cast_send("cast", f + 1, i, f - 1)
+        else:
+            cast_arrive(over, i)
+            cast_send("cast2", over, i, (nf - 1) * (f - 1))
 
     @pl.when(inner)
     def _():
-        for i in range(2):
+        for i in range(LEAVES):
             cast_send("cast", f, i, f - 1)
             cast_send("cast", f, i, f + 1)
 
     @pl.when(jnp.logical_not(inner))
     def _():
-        for i in range(2):
+        for i in range(LEAVES):
             cast_send("cast", f, i, place(0))
 
+    settle(load_sem.at[nr], c_ref)
     send("twin", "twin", c_ref, c_twin, (f, r, 1 - t))
-    for j in range(2, nf):
+    ready(3)
+    for j in range(nf):
         fill(3, j)
     send_open(0, 0)
     send_open(1, 0)
@@ -307,16 +309,15 @@
     ready(0)
     for j in range(nf):
         fill(0, j)
-    relay(1, 0)
+    relay(1, range(LEAVES))
     send_second(0)
-    send_first(2)
 
     def cast(q):
         where = pl.ds(pl.multiple_of(q * nr * thin, nr * thin), nr * thin)
         return jnp.dot(x_ref[:, where], p_all[q], preferred_element_type=fl)
 
     xp_ref[...] = cast(f)
-    relay(1, 1)
+    relay(2, range(LEAVES))
 
     for i, ref in enumerate((gc_ref, gt_ref, lm_ref, ls_ref)):
         settle(load_sem.at[nr + 2 + i], ref)
@@ -350,32 +351,27 @@
         for j in range(nf):
             start = (i * nf + j) * thin
             ra_send[i, j] = gate_partial[:, start : start + thin]
-    for k in squares:
-        send("ra", "ra", ra_send.at[square[k]], ra_recv.at[k - 1], rep(k))
-
-    relay(2, 0)
-    send_second(1)
-    relay(2, 1)
-    send_third(0)
 
     def arrive_cast(n):
         @pl.when(jnp.logical_not(inner))
         def _():
-            for i in range(2):
+            for i in range(LEAVES):
                 cast_arrive(place(n), i)
         return cast(place(n))
 
     xp_ref[...] += arrive_cast(0)
     xp_ref[...] += arrive_cast(1)
+    send_second(1)
+    send_first(2)
     cast_all = xp_ref[...] + arrive_cast(2)
     high = cast_all.astype(bf)
     low = (cast_all - high.astype(fl)).astype(bf)
+    terms = jnp.concatenate([high, low], axis=1)
     arrive("twin", c_twin)
     crossed = lax.rem(line + t, 2)
     for u, ref in ((1, c_twin), (0, c_ref)):
-        partial = lax.dot_general(high, ref[...], CONTRACT, preferred_element_type=fl)
-        partial += lax.dot_general(low, ref[...], CONTRACT, preferred_element_type=fl)
-        partial = (partial * norming).astype(bf)
+        partial = lax.dot_general(terms, ref[...], CONTRACT, preferred_element_type=fl)
+        partial = ((partial[:rank_half] + partial[rank_half:]) * norming).astype(bf)
         straight, across = partial[:rank_rows], partial[rank_rows:]
         d_send[0, u] = jnp.where(side == 0, straight, across)
         d_send[1, u] = jnp.where(side == 0, across, straight)
@@ -394,35 +390,39 @@
             def _():
                 send("d1", "d", d_send.at[0, 0], d_recv.at[2], rep(2))
 
+    send_third(0)
+    send_third(1)
+    send_first(3)
     send_second(2)
-    send_first(3)
+    for k in squares:
+        send("ra", "ra", ra_send.at[square[k]], ra_recv.at[k - 1], rep(k))
     send_cross(0)
-    send_third(1)
+    send_cross(1)
+
+    @pl.when(crossed == 0)
+    def _():
+        arrive("d", d_recv.at[: nr - 1])
+
+    @pl.when(crossed == 1)
+    def _():
+        arrive("d", d_recv)
+
+    total = d_recv[0].astype(fl)
+    for k in squares:
+        total = total + d_recv[k].astype(fl)
+    e_all[f] = total.astype(bf)
+    spread("e", "e", e_all.at[f], e_all.at[f])
+    send_second(3)
+    send_fourth(0)
+    send_third(2)
+    send_fourth(1)
     arrive("ra", ra_recv)
     gate_rows = ra_send[r]
     for k in squares:
         gate_rows = gate_rows + ra_recv[k - 1]
     rb_all[f] = gate_rows
     spread("rb", "rb", rb_all.at[f], rb_all.at[f])
-
-    @pl.when(crossed == 0)
-    def _():
-        arrive("d", d_recv.at[: nr - 1])
-
-    @pl.when(crossed == 1)
-    def _():
-        arrive("d", d_recv)
-
-    total = d_recv[0].astype(fl)
-    for k in squares:
-        total = total + d_recv[k].astype(fl)
-    e_all[f] = total.astype(bf)
-    spread("e", "e", e_all.at[f], e_all.at[f])
-    send_cross(1)
-    send_fourth(0)
-    send_third(2)
-    send_second(3)
-    send_cross(2)
+    send_third(3)
 
     arrive("e", e_all.at[: nf - 1])
     projected = e_all[0].astype(fl)
@@ -436,8 +436,16 @@
     for i, spot in enumerate(spots):
         send("f", "f", f_send, f_recv.at[i], spot)
     projected_ref[...] = projected
-    send_fourth(1)
-    send_third(3)
+    send_cross(2)
+    send_cross(3)
+    arrive("rb", rb_all.at[: nf - 1])
+    gate_block = rb_all[0]
+    for j in fss:
+        gate_block = gate_block + rb_all[j]
+    rd_all[r] = gate_block * norming
+    for k in squares:
+        send("rd", "rd", rd_all.at[r], rd_all.at[r], rep(k))
+    send_fourth(2)
     arrive("f", f_recv)
     sums = f_send[...]
     for i in range(len(spots)):
@@ -448,15 +456,6 @@
     for k in squares:
         send("h", "h", h_all.at[r], h_all.at[r], rep(k))
 
-    send_fourth(2)
-    arrive("rb", rb_all.at[: nf - 1])
-    gate_block = rb_all[0]
-    for j in fss:
-        gate_block = gate_block + rb_all[j]
-    rd_all[r] = gate_block * norming
-    for k in squares:
-        send("rd", "rd", rd_all.at[r], rd_all.at[r], rep(k))
-    send_cross(3)
     send_fourth(3)
     arrive("rd", rd_all.at[: nr - 1])
     arrive("h", h_all.at[: nr - 1])
@@ -486,36 +485,55 @@
 
 def closing_kernel(
     g_ref, h_ref, balance_ref, projected_ref, gate_ref, pj_ref, qm_ref, lm_ref, ls_ref, gm_ref, gq_ref,
-    qu_ref, qr_ref, qc_ref, ma_ref, sa_ref, gu_ref, ga_ref, ge_ref,
+    *rest,
 ):
-    lifted = jnp.dot(
-        pj_ref[...], h_ref[...].reshape(pj_ref.shape[1], qm_ref.shape[1]),
-        preferred_element_type=jnp.float32,
-    )
-    query_update = lifted + balance_ref[:1, :1] * g_ref[0].astype(jnp.float32)
-    query_renewed = qm_ref[...] - STEP_RATE * query_update
-    qu_ref[...] = query_update
-    qr_ref[...] = query_renewed
-    qc_ref[...] = query_renewed.astype(jnp.bfloat16)
-
-    @pl.when(pl.program_id(0) == 0)
-    def _():
-        projected = projected_ref[...]
-        ma_ref[...] = BETA_ONE * lm_ref[...] + (1.0 - BETA_ONE) * projected
-        sa_ref[...] = BETA_TWO * ls_ref[...] + (1.0 - BETA_TWO) * projected * projected
-        nr, nf, _, thin = gate_ref.shape
-        for i in range(nr):
-            for j in range(nf):
-                window = slice((i * nf + j) * thin, (i * nf + j + 1) * thin)
-                forget_gradient = gate_ref[i, j]
-                average = BETA_ONE * gm_ref[:, window] + (1.0 - BETA_ONE) * forget_gradient
-                energy = (
-                    BETA_TWO * gq_ref[:, window]
-                    + (1.0 - BETA_TWO) * forget_gradient * forget_gradient
-                )
-                ga_ref[:, window] = average
-                ge_ref[:, window] = energy
-                gu_ref[:, window] = average / (jnp.sqrt(energy) + EPSILON)
+    outs, staged, out_sem = rest[:8], rest[8:16], rest[16]
+    qu_ref, qr_ref, qc_ref, ma_ref, sa_ref, gu_ref, ga_ref, ge_ref = staged
+    copies = []
+
+    def flush(i, where=slice(None)):
+        copy = pltpu.make_async_copy(
+            staged[i].at[where], outs[i].at[where], out_sem.at[len(copies)]
+        )
+        copy.start()
+        copies.append(copy)
+
+    factor = h_ref[...].reshape(pj_ref.shape[1], qm_ref.shape[1])
+    balance = balance_ref[:1, :1]
+    thin = g_ref.shape[1]
+    for i in range(g_ref.shape[0]):
+        rows = slice(i * thin, (i + 1) * thin)
+        lifted = jnp.dot(pj_ref[rows], factor, preferred_element_type=jnp.float32)
+        query_update = lifted + balance * g_ref[i].astype(jnp.float32)
+        query_renewed = qm_ref[rows] - STEP_RATE * query_update
+        qu_ref[rows] = query_update
+        flush(0, rows)
+        qr_ref[rows] = query_renewed
+        flush(1, rows)
+        qc_ref[rows] = query_renewed.astype(jnp.bfloat16)
+        flush(2, rows)
+    projected = projected_ref[...]
+    ma_ref[...] = BETA_ONE * lm_ref[...] + (1.0 - BETA_ONE) * projected
+    flush(3)
+    sa_ref[...] = BETA_TWO * ls_ref[...] + (1.0 - BETA_TWO) * projected * projected
+    flush(4)
+    nr, nf, _, thin = gate_ref.shape
+    for i in range(nr):
+        for j in range(nf):
+            window = slice((i * nf + j) * thin, (i * nf + j + 1) * thin)
+            forget_gradient = gate_ref[i, j]
+            average = BETA_ONE * gm_ref[:, window] + (1.0 - BETA_ONE) * forget_gradient
+            energy = (
+                BETA_TWO * gq_ref[:, window]
+                + (1.0 - BETA_TWO) * forget_gradient * forget_gradient
+            )
+            ga_ref[:, window] = average
+            ge_ref[:, window] = energy
+            gu_ref[:, window] = average / (jnp.sqrt(energy) + EPSILON)
+    for i in (5, 6, 7):
+        flush(i)
+    for copy in copies:
+        copy.wait()
 
 
 def per_device(nf, nr, nt, *args):
@@ -525,7 +543,7 @@
     thin = width // (nf * nr)
     fits = (
         width % (nf * nr * 128) == 0 and rank_rows % 16 == 0
-        and cols % (PIECES * 128) == 0 and heads % 8 == 0 and nf == 4 and nr == 4 and nt == 2
+        and cols % (PIECES * 128) == 0 and heads % 8 == 0 and nf == 4 and nr == 4 and nr * thin % (LEAVES * 16) == 0 and nt == 2
         and x.shape[0] % 128 == 0 and rank_all % (nt * 128) == 0
     )
     if not fits:
@@ -555,7 +573,7 @@
     ]
     vmem = pl.BlockSpec(memory_space=pltpu.VMEM)
     hbm = pl.BlockSpec(memory_space=pltpu.HBM)
-    semaphores = (16, 4 * PIECES + 10 + 2 * nf, nr + 6)
+    semaphores = (16, 4 * PIECES + 10 + LEAVES * nf, nr + 6)
     passed = pl.pallas_call(
         functools.partial(fused_kernel, nf, nr, nt),
         out_shape=tuple(jax.ShapeDtypeStruct(*o) for o in between),
@@ -568,22 +586,14 @@
         ),
     )(*(pltpu.with_memory_space_constraint(v, pltpu.HBM) for v in (x, c, gc, gt, pj, lm, ls)))
 
-    def whole(shape):
-        return pl.BlockSpec(shape, lambda i: (0,) * len(shape))
-
-    def rows(width):
-        return pl.BlockSpec((thin, width), lambda i: (i, 0))
-
     return pl.pallas_call(
         closing_kernel,
-        grid=(nr,),
         out_shape=tuple(jax.ShapeDtypeStruct(*o) for o in outs),
-        in_specs=[pl.BlockSpec((1, thin, cols), lambda i: (i, 0, 0))]
-        + [whole(b[0]) for b in between[1:]]
-        + [rows(pj.shape[1]), rows(cols), whole(lm.shape), whole(ls.shape)]
-        + [whole(gm.shape), whole(gq.shape)],
-        out_specs=(rows(cols),) * 3 + tuple(whole(o[0]) for o in outs[3:]),
-        compiler_params=pltpu.CompilerParams(vmem_limit_bytes=VMEM_GRANT),
+        in_specs=[vmem] * (len(between) + 6),
+        out_specs=(hbm,) * len(outs),
+        scratch_shapes=[pltpu.VMEM(*o) for o in outs]
+        + [pltpu.SemaphoreType.DMA((3 * nr + 5,))],
+        compiler_params=pltpu.CompilerParams(vmem_limit_bytes=VMEM_GRANT // 2),
     )(*passed, pj, qm, lm, ls, gm, gq)
 
 

time: 47.6 us -> 46.1 us (0.968)
  Pallas kernels: 46.7 us -> 45.2 us
    pallas_call x1, Pallas kernels: 44.1 us -> 43.2 us  [per_device(): pl.pallas_call(functools.partial(fused_kernel, nf, nr, nt), out_shape=tup...]
    pallas_call x1, Pallas kernels: 2.64 us -> 1.99 us  [per_device(): pl.pallas_call(closing_kernel, out_shape=tuple((jax.ShapeDtypeStruct(*o)...]
where the time goes in v7:
time: 46.1 us; the launch traced here: 46 us
  Pallas kernels  45.2 us (98%)
  between operations  0.74 us (2%)
    pallas_call x1, Pallas kernels, per_device(): pl.pallas_call(functools.partial(fused_kernel, nf, nr, nt), out_shape=tup...  43.2 us
    pallas_call x1, Pallas kernels, per_device(): pl.pallas_call(closing_kernel, out_shape=tuple((jax.ShapeDtypeStruct(*o)...  1.99 us

profile of v7, /device:TPU:0, one launch (start us, length us, event | category | flops | bytes accessed | tf_op | source)
XLA Modules:
  0.0 46.0 jit_solution(12468671479401390203)
XLA Ops:
  0.6 0.0 copy-start.3
  0.6 0.0 copy-start.2
  0.7 0.0 copy-start.1
  0.7 0.0 copy-start.5
  0.7 0.0 copy-start.4
  0.7 0.0 copy-start
  0.7 43.2 %shard_map.161 = (bf16[4,128,512]{2,1,0:T(8,128)(2,1)S(1)}, bf16[4,64,512]{2,1,0:T(8,128)(2,1)S(1)}, f32[8,128]{1,0:T(8,128)S(1)}, f32[64,512]{1,0:T(8,128)S(1)}, f32[4,4,8,128]{3,2,1,0:T(8,128)S(1)}) custom-call(bf16[768,2048]{1,0:T(8,128)(2,1)} %x_hbm.1, bf16[768,512]{1,0:T(8,128)(2,1)} %c_hbm.1, f32[8,768]{1,0:T(8,128)} %gc_hbm.1, f32[8,768]{1,0:T(8,128)} %gt_hbm.1, ...), custom_call_target="tpu_custom_call" | custom-call | tf_op jit(solution)/shard_map/pallas_call | solution.py:577
  43.9 0.0 copy-done.3
  43.9 0.0 copy-done.2
  43.9 0.0 copy-done.1
  44.0 0.0 copy-done.5
  44.0 0.0 copy-done.4
  44.0 0.0 copy-done
  44.0 2.0 %shard_map.162 = (f32[512,512]{1,0:T(8,128)}, f32[512,512]{1,0:T(8,128)}, bf16[512,512]{1,0:T(8,128)(2,1)}, f32[64,512]{1,0:T(8,128)}, f32[64,512]{1,0:T(8,128)}...) custom-call(bf16[4,128,512]{2,1,0:T(8,128)(2,1)S(1)} %get-tuple-element.13.g_ref, ...), custom_call_target="tpu_custom_call" | custom-call | tf_op jit(solution)/shard_map/pallas_call | solution.py:589
Async XLA Ops:
  0.6 43.3 %copy-start.3 = (f32[64,512]{1,0:T(8,128)S(1)}, f32[64,512]{1,0:T(8,128)}, u32[]{:S(2)}) copy-start(f32[64,512]{1,0:T(8,128)} %ls_ref.1) | copy-start | bytes 393220
  0.6 43.3 %copy-start.2 = (f32[64,512]{1,0:T(8,128)S(1)}, f32[64,512]{1,0:T(8,128)}, u32[]{:S(2)}) copy-start(f32[64,512]{1,0:T(8,128)} %lm_ref.1) | copy-start | bytes 393220
  0.7 43.3 %copy-start.1 = (bf16[512,256]{1,0:T(8,128)(2,1)S(1)}, bf16[512,256]{1,0:T(8,128)(2,1)}, u32[]{:S(2)}) copy-start(bf16[512,256]{1,0:T(8,128)(2,1)} %pj_ref.1) | copy-start | bytes 786436
  0.7 43.3 %copy-start.5 = (f32[8,2048]{1,0:T(8,128)S(1)}, f32[8,2048]{1,0:T(8,128)}, u32[]{:S(2)}) copy-start(f32[8,2048]{1,0:T(8,128)} %gq_ref.1) | copy-start | bytes 196612
  0.7 43.3 %copy-start.4 = (f32[8,2048]{1,0:T(8,128)S(1)}, f32[8,2048]{1,0:T(8,128)}, u32[]{:S(2)}) copy-start(f32[8,2048]{1,0:T(8,128)} %gm_ref.1) | copy-start | bytes 196612
  0.7 43.3 %copy-start = (f32[512,512]{1,0:T(8,128)S(1)}, f32[512,512]{1,0:T(8,128)}, u32[]{:S(2)}) copy-start(f32[512,512]{1,0:T(8,128)} %qm_ref.1) | copy-start | bytes 3145732

commit v8 on v7

--- a/solution.py
+++ b/solution.py
@@ -229,7 +229,14 @@
         for o, j in enumerate((mate_over, mate)):
             for h in range(2):
                 b_send[p, o, h] = summed(p, h, j).astype(bf)
-        send("third", ("third", p), b_send.at[p], b_recv.at[p], (mate, r, t))
+        if p < PIECES - 1:
+            send("third", ("third", p), b_send.at[p], b_recv.at[p], (mate, r, t))
+            return
+        for h in range(2):
+            v_send[p, h] = summed(p, h, over).astype(bf)
+        send("third", ("third", p), b_send.at[p, 0], b_recv.at[p, 0], (mate_over, r, t))
+        send("cross", ("cross", p), v_send.at[p], v_recv.at[p], (over, r, t))
+        send("third", ("third", p), b_send.at[p, 1], b_recv.at[p, 1], (mate, r, t))
 
     def send_cross(p):
         arrive(("third", p), b_recv.at[p])
@@ -239,11 +246,15 @@
 
     def send_fourth(p):
         arrive(("cross", p), v_recv.at[p])
+        if p == PIECES - 1:
+            arrive(("third", p), b_recv.at[p])
         for h in range(2):
             total = summed(p, h, f) + b_recv[p, 1, h].astype(fl) + v_recv[p, h].astype(fl)
+            if p == PIECES - 1:
+                total = total + b_recv[p, 0, h].astype(fl)
             g_all[r, h * half : (h + 1) * half, cut(p)] = (total * norming).astype(bf)
         where = g_all.at[r, :, cut(p)]
-        for k in squares:
+        for k in (3, 1, 2):
             send("fourth", "fourth", where, where, rep(k))
 
     settle(load_sem.at[nr + 1], p_all.at[0])
@@ -359,6 +370,8 @@
                 cast_arrive(place(n), i)
         return cast(place(n))
 
+    for k in (3, 1, 2):
+        send("ra", "ra", ra_send.at[square[k]], ra_recv.at[k - 1], rep(k))
     xp_ref[...] += arrive_cast(0)
     xp_ref[...] += arrive_cast(1)
     send_second(1)
@@ -391,38 +404,36 @@
                 send("d1", "d", d_send.at[0, 0], d_recv.at[2], rep(2))
 
     send_third(0)
-    send_third(1)
-    send_first(3)
-    send_second(2)
-    for k in squares:
-        send("ra", "ra", ra_send.at[square[k]], ra_recv.at[k - 1], rep(k))
-    send_cross(0)
-    send_cross(1)
-
-    @pl.when(crossed == 0)
-    def _():
-        arrive("d", d_recv.at[: nr - 1])
-
-    @pl.when(crossed == 1)
-    def _():
-        arrive("d", d_recv)
-
-    total = d_recv[0].astype(fl)
-    for k in squares:
-        total = total + d_recv[k].astype(fl)
-    e_all[f] = total.astype(bf)
-    spread("e", "e", e_all.at[f], e_all.at[f])
-    send_second(3)
-    send_fourth(0)
-    send_third(2)
-    send_fourth(1)
     arrive("ra", ra_recv)
     gate_rows = ra_send[r]
     for k in squares:
         gate_rows = gate_rows + ra_recv[k - 1]
     rb_all[f] = gate_rows
     spread("rb", "rb", rb_all.at[f], rb_all.at[f])
-    send_third(3)
+    send_third(1)
+    send_second(2)
+    send_first(3)
+    send_cross(0)
+    send_cross(1)
+
+    @pl.when(crossed == 0)
+    def _():
+        arrive("d", d_recv.at[: nr - 1])
+
+    @pl.when(crossed == 1)
+    def _():
+        arrive("d", d_recv)
+
+    total = d_recv[0].astype(fl)
+    for k in squares:
+        total = total + d_recv[k].astype(fl)
+    e_all[f] = total.astype(bf)
+    spread("e", "e", e_all.at[f], e_all.at[f])
+    send_fourth(0)
+    send_third(2)
+    send_second(3)
+    send_fourth(1)
+    send_cross(2)
 
     arrive("e", e_all.at[: nf - 1])
     projected = e_all[0].astype(fl)
@@ -436,14 +447,13 @@
     for i, spot in enumerate(spots):
         send("f", "f", f_send, f_recv.at[i], spot)
     projected_ref[...] = projected
-    send_cross(2)
-    send_cross(3)
+    send_third(3)
     arrive("rb", rb_all.at[: nf - 1])
     gate_block = rb_all[0]
     for j in fss:
         gate_block = gate_block + rb_all[j]
     rd_all[r] = gate_block * norming
-    for k in squares:
+    for k in (3, 1, 2):
         send("rd", "rd", rd_all.at[r], rd_all.at[r], rep(k))
     send_fourth(2)
     arrive("f", f_recv)
@@ -453,7 +463,7 @@
     balance = jnp.sqrt(sums[:1, :1] / (sums[1:2, :1] + NORM_FLOOR))
     balance_ref[...] = jnp.broadcast_to(balance, balance_ref.shape)
     h_all[r] = (direction - balance * projected).astype(bf)
-    for k in squares:
+    for k in (3, 1, 2):
         send("h", "h", h_all.at[r], h_all.at[r], rep(k))
 
     send_fourth(3)

time: 46.1 us -> 45.4 us (0.985)
  Pallas kernels: 45.2 us -> 44.4 us
    pallas_call x1, Pallas kernels: 43.2 us -> 42.4 us  [per_device(): pl.pallas_call(functools.partial(fused_kernel, nf, nr, nt), out_shape=tup...]
where the time goes in v8:
time: 45.4 us; the launch traced here: 45.2 us
  Pallas kernels  44.4 us (98%)
  between operations  0.74 us (2%)
    pallas_call x1, Pallas kernels, per_device(): pl.pallas_call(functools.partial(fused_kernel, nf, nr, nt), out_shape=tup...  42.4 us
    pallas_call x1, Pallas kernels, per_device(): pl.pallas_call(closing_kernel, out_shape=tuple((jax.ShapeDtypeStruct(*o)...  2.01 us

profile of v8, /device:TPU:0, one launch (start us, length us, event | category | flops | bytes accessed | tf_op | source)
XLA Modules:
  0.0 45.2 jit_solution(18366618452256084505)
XLA Ops:
  0.6 0.0 copy-start.3
  0.6 0.0 copy-start.2
  0.7 0.0 copy-start.1
  0.7 0.0 copy-start.5
  0.7 0.0 copy-start.4
  0.7 0.0 copy-start
  0.7 42.4 %shard_map.161 = (bf16[4,128,512]{2,1,0:T(8,128)(2,1)S(1)}, bf16[4,64,512]{2,1,0:T(8,128)(2,1)S(1)}, f32[8,128]{1,0:T(8,128)S(1)}, f32[64,512]{1,0:T(8,128)S(1)}, f32[4,4,8,128]{3,2,1,0:T(8,128)S(1)}) custom-call(bf16[768,2048]{1,0:T(8,128)(2,1)} %x_hbm.1, bf16[768,512]{1,0:T(8,128)(2,1)} %c_hbm.1, f32[8,768]{1,0:T(8,128)} %gc_hbm.1, f32[8,768]{1,0:T(8,128)} %gt_hbm.1, ...), custom_call_target="tpu_custom_call" | custom-call | tf_op jit(solution)/shard_map/pallas_call | solution.py:587
  43.1 0.0 copy-done.3
  43.2 0.0 copy-done.2
  43.2 0.0 copy-done.1
  43.2 0.0 copy-done.5
  43.2 0.0 copy-done.4
  43.2 0.0 copy-done
  43.2 2.0 %shard_map.162 = (f32[512,512]{1,0:T(8,128)}, f32[512,512]{1,0:T(8,128)}, bf16[512,512]{1,0:T(8,128)(2,1)}, f32[64,512]{1,0:T(8,128)}, f32[64,512]{1,0:T(8,128)}...) custom-call(bf16[4,128,512]{2,1,0:T(8,128)(2,1)S(1)} %get-tuple-element.13.g_ref, ...), custom_call_target="tpu_custom_call" | custom-call | tf_op jit(solution)/shard_map/pallas_call | solution.py:599
Async XLA Ops:
  0.6 42.5 %copy-start.3 = (f32[64,512]{1,0:T(8,128)S(1)}, f32[64,512]{1,0:T(8,128)}, u32[]{:S(2)}) copy-start(f32[64,512]{1,0:T(8,128)} %ls_ref.1) | copy-start | bytes 393220
  0.6 42.5 %copy-start.2 = (f32[64,512]{1,0:T(8,128)S(1)}, f32[64,512]{1,0:T(8,128)}, u32[]{:S(2)}) copy-start(f32[64,512]{1,0:T(8,128)} %lm_ref.1) | copy-start | bytes 393220
  0.7 42.5 %copy-start.1 = (bf16[512,256]{1,0:T(8,128)(2,1)S(1)}, bf16[512,256]{1,0:T(8,128)(2,1)}, u32[]{:S(2)}) copy-start(bf16[512,256]{1,0:T(8,128)(2,1)} %pj_ref.1) | copy-start | bytes 786436
  0.7 42.5 %copy-start.5 = (f32[8,2048]{1,0:T(8,128)S(1)}, f32[8,2048]{1,0:T(8,128)}, u32[]{:S(2)}) copy-start(f32[8,2048]{1,0:T(8,128)} %gq_ref.1) | copy-start | bytes 196612
  0.7 42.5 %copy-start.4 = (f32[8,2048]{1,0:T(8,128)S(1)}, f32[8,2048]{1,0:T(8,128)}, u32[]{:S(2)}) copy-start(f32[8,2048]{1,0:T(8,128)} %gm_ref.1) | copy-start | bytes 196612
  0.7 42.5 %copy-start = (f32[512,512]{1,0:T(8,128)S(1)}, f32[512,512]{1,0:T(8,128)}, u32[]{:S(2)}) copy-start(f32[512,512]{1,0:T(8,128)} %qm_ref.1) | copy-start | bytes 3145732

commit v9 on v8

--- a/solution.py
+++ b/solution.py
@@ -260,7 +260,7 @@
     settle(load_sem.at[nr + 1], p_all.at[0])
     pl.semaphore_wait(barrier, len(peers))
     inner = f * (nf - 1 - f) > 0
-    cast_sem = 4 * PIECES + 10
+    cast_sem = 4 * PIECES + 11
     deep = p_all.shape[1] // LEAVES
 
     def leaf(q, i):
@@ -382,26 +382,34 @@
     terms = jnp.concatenate([high, low], axis=1)
     arrive("twin", c_twin)
     crossed = lax.rem(line + t, 2)
+    short = rank_rows // 2
+
+    def send_d(u, i):
+        core = lax.rem(t + u, nt)
+        near = (f, (1 - crossed) * square[0] + crossed * square[2], core)
+        far = (f, (1 - crossed) * square[1] + crossed * square[3], core)
+        own = slice(i * short, (i + 1) * short)
+        send("d", ("d", i), d_send.at[1, u, own], d_recv.at[i, 1 + 2 * crossed], far)
+        if u == 1:
+            send("d", ("d", i), d_send.at[0, u, own], d_recv.at[i, 2 * crossed], near)
+        else:
+            @pl.when(crossed == 0)
+            def _():
+                d_recv[i, 0] = d_send[0, 0, own]
+
+            @pl.when(crossed == 1)
+            def _():
+                send("d1", ("d", i), d_send.at[0, 0, own], d_recv.at[i, 2], rep(2))
+
     for u, ref in ((1, c_twin), (0, c_ref)):
         partial = lax.dot_general(terms, ref[...], CONTRACT, preferred_element_type=fl)
         partial = ((partial[:rank_half] + partial[rank_half:]) * norming).astype(bf)
         straight, across = partial[:rank_rows], partial[rank_rows:]
         d_send[0, u] = jnp.where(side == 0, straight, across)
         d_send[1, u] = jnp.where(side == 0, across, straight)
-        core = lax.rem(t + u, nt)
-        near = (f, (1 - crossed) * square[0] + crossed * square[2], core)
-        far = (f, (1 - crossed) * square[1] + crossed * square[3], core)
-        send("d", "d", d_send.at[1, u], d_recv.at[1 + 2 * crossed], far)
-        if u == 1:
-            send("d", "d", d_send.at[0, u], d_recv.at[2 * crossed], near)
-        else:
-            @pl.when(crossed == 0)
-            def _():
-                d_recv[0] = d_send[0, 0]
-
-            @pl.when(crossed == 1)
-            def _():
-                send("d1", "d", d_send.at[0, 0], d_recv.at[2], rep(2))
+        send_d(u, 0)
+    for u in (1, 0):
+        send_d(u, 1)
 
     send_third(0)
     arrive("ra", ra_recv)
@@ -416,19 +424,21 @@
     send_cross(0)
     send_cross(1)
 
-    @pl.when(crossed == 0)
-    def _():
-        arrive("d", d_recv.at[: nr - 1])
-
-    @pl.when(crossed == 1)
-    def _():
-        arrive("d", d_recv)
-
-    total = d_recv[0].astype(fl)
-    for k in squares:
-        total = total + d_recv[k].astype(fl)
-    e_all[f] = total.astype(bf)
-    spread("e", "e", e_all.at[f], e_all.at[f])
+    for i in range(2):
+        @pl.when(crossed == 0)
+        def _():
+            arrive(("d", i), d_recv.at[i, : nr - 1])
+
+        @pl.when(crossed == 1)
+        def _():
+            arrive(("d", i), d_recv.at[i])
+
+        total = d_recv[i, 0].astype(fl)
+        for k in squares:
+            total = total + d_recv[i, k].astype(fl)
+        own = slice(i * short, (i + 1) * short)
+        e_all[f, own] = total.astype(bf)
+        spread("e", "e", e_all.at[f, own], e_all.at[f, own])
     send_fourth(0)
     send_third(2)
     send_second(3)
@@ -472,7 +482,7 @@
     arrive("fourth", g_all.at[: nr - 1])
     sent = {
         "first": a_send, "twin": c_ref, "second": m_send,
-        "third": b_send, "cross": v_send, "fourth": g_all.at[: nr - 1], "d": d_recv.at[: nr - 1],
+        "third": b_send, "cross": v_send, "fourth": g_all.at[: nr - 1], "d": e_all.at[: nf - 1],
         "e": e_all.at[: nf - 1], "f": f_recv, "h": h_all.at[: nr - 1], "ra": ra_recv,
         "rb": rb_all.at[: nf - 1], "rd": rd_all.at[: nr - 1],
     }
@@ -552,7 +562,7 @@
     rank_all = pj.shape[1]
     thin = width // (nf * nr)
     fits = (
-        width % (nf * nr * 128) == 0 and rank_rows % 16 == 0
+        width % (nf * nr * 128) == 0 and rank_rows % 32 == 0
         and cols % (PIECES * 128) == 0 and heads % 8 == 0 and nf == 4 and nr == 4 and nr * thin % (LEAVES * 16) == 0 and nt == 2
         and x.shape[0] % 128 == 0 and rank_all % (nt * 128) == 0
     )
@@ -568,7 +578,7 @@
         ((PIECES, 2, 2, half, piece), bf), ((PIECES, 2, 2, half, piece), bf),
         ((PIECES, 2, half, piece), bf), ((PIECES, 2, half, piece), bf),
         ((x.shape[0], rank_all // nt), fl),
-        ((2, nt, rank_rows, cols), bf), ((nr, rank_rows, cols), bf),
+        ((2, nt, rank_rows, cols), bf), ((2, nr, rank_rows // 2, cols), bf),
         ((nf, rank_rows, cols), bf), ((8, 128), fl), ((nr * nt - 1, 8, 128), fl),
         ((nr, nf, heads, thin), fl), ((nr - 1, nf, heads, thin), fl),
         ((nf, nf, heads, thin), fl),
@@ -583,7 +593,7 @@
     ]
     vmem = pl.BlockSpec(memory_space=pltpu.VMEM)
     hbm = pl.BlockSpec(memory_space=pltpu.HBM)
-    semaphores = (16, 4 * PIECES + 10 + LEAVES * nf, nr + 6)
+    semaphores = (16, 4 * PIECES + 11 + LEAVES * nf, nr + 6)
     passed = pl.pallas_call(
         functools.partial(fused_kernel, nf, nr, nt),
         out_shape=tuple(jax.ShapeDtypeStruct(*o) for o in between),

time: 45.4 us -> 45.7 us (level)
  no operation moved by 1% of the time
where the time goes in v9:
time: 45.7 us; the launch traced here: 45.6 us
  Pallas kernels  44.8 us (98%)
  between operations  0.74 us (2%)
    pallas_call x1, Pallas kernels, per_device(): pl.pallas_call(functools.partial(fused_kernel, nf, nr, nt), out_shape=tup...  42.8 us
    pallas_call x1, Pallas kernels, per_device(): pl.pallas_call(closing_kernel, out_shape=tuple((jax.ShapeDtypeStruct(*o)...  1.99 us

profile of v9, /device:TPU:0, one launch (start us, length us, event | category | flops | bytes accessed | tf_op | source)
XLA Modules:
  0.0 45.6 jit_solution(17030829046152452308)
XLA Ops:
  0.6 0.0 copy-start.3
  0.6 0.0 copy-start.2
  0.7 0.0 copy-start.1
  0.7 0.0 copy-start.5
  0.7 0.0 copy-start.4
  0.7 0.0 copy-start
  0.7 42.8 %shard_map.161 = (bf16[4,128,512]{2,1,0:T(8,128)(2,1)S(1)}, bf16[4,64,512]{2,1,0:T(8,128)(2,1)S(1)}, f32[8,128]{1,0:T(8,128)S(1)}, f32[64,512]{1,0:T(8,128)S(1)}, f32[4,4,8,128]{3,2,1,0:T(8,128)S(1)}) custom-call(bf16[768,2048]{1,0:T(8,128)(2,1)} %x_hbm.1, bf16[768,512]{1,0:T(8,128)(2,1)} %c_hbm.1, f32[8,768]{1,0:T(8,128)} %gc_hbm.1, f32[8,768]{1,0:T(8,128)} %gt_hbm.1, ...), custom_call_target="tpu_custom_call" | custom-call | tf_op jit(solution)/shard_map/pallas_call | solution.py:597
  43.5 0.0 copy-done.3
  43.5 0.0 copy-done.2
  43.6 0.0 copy-done.1
  43.6 0.0 copy-done.5
  43.6 0.0 copy-done.4
  43.6 0.0 copy-done
  43.6 2.0 %shard_map.162 = (f32[512,512]{1,0:T(8,128)}, f32[512,512]{1,0:T(8,128)}, bf16[512,512]{1,0:T(8,128)(2,1)}, f32[64,512]{1,0:T(8,128)}, f32[64,512]{1,0:T(8,128)}...) custom-call(bf16[4,128,512]{2,1,0:T(8,128)(2,1)S(1)} %get-tuple-element.13.g_ref, ...), custom_call_target="tpu_custom_call" | custom-call | tf_op jit(solution)/shard_map/pallas_call | solution.py:609
Async XLA Ops:
  0.6 42.9 %copy-start.3 = (f32[64,512]{1,0:T(8,128)S(1)}, f32[64,512]{1,0:T(8,128)}, u32[]{:S(2)}) copy-start(f32[64,512]{1,0:T(8,128)} %ls_ref.1) | copy-start | bytes 393220
  0.6 42.9 %copy-start.2 = (f32[64,512]{1,0:T(8,128)S(1)}, f32[64,512]{1,0:T(8,128)}, u32[]{:S(2)}) copy-start(f32[64,512]{1,0:T(8,128)} %lm_ref.1) | copy-start | bytes 393220
  0.7 42.9 %copy-start.1 = (bf16[512,256]{1,0:T(8,128)(2,1)S(1)}, bf16[512,256]{1,0:T(8,128)(2,1)}, u32[]{:S(2)}) copy-start(bf16[512,256]{1,0:T(8,128)(2,1)} %pj_ref.1) | copy-start | bytes 786436
  0.7 42.9 %copy-start.5 = (f32[8,2048]{1,0:T(8,128)S(1)}, f32[8,2048]{1,0:T(8,128)}, u32[]{:S(2)}) copy-start(f32[8,2048]{1,0:T(8,128)} %gq_ref.1) | copy-start | bytes 196612
  0.7 42.9 %copy-start.4 = (f32[8,2048]{1,0:T(8,128)S(1)}, f32[8,2048]{1,0:T(8,128)}, u32[]{:S(2)}) copy-start(f32[8,2048]{1,0:T(8,128)} %gm_ref.1) | copy-start | bytes 196612
  0.7 42.9 %copy-start = (f32[512,512]{1,0:T(8,128)S(1)}, f32[512,512]{1,0:T(8,128)}, u32[]{:S(2)}) copy-start(f32[512,512]{1,0:T(8,128)} %qm_ref.1) | copy-start | bytes 3145732
